TPU v7x, 128 devices: a whole 4x4x4 slice. The times are simulated.
128 devices in a mesh: rep: 2 (over z_hi), fs: 32 (over z_lo, y, x), tp: 2 (over core).
Axes of the slice: x: 4, y: 4, z: 4 (z_hi: 2, z_lo: 2; z = z_hi * 2 + z_lo), core: 2. Of those that a mesh axis runs over, the one named last changes fastest.
Arguments:
- resid: bfloat16 [49152, 2048], P(('rep', 'fs', 'tp')), may hold values from -6 to 6
- mix_gain: float32 [2048], replicated, may hold values from 0.1 to 1.9
- query_weight: bfloat16 [2048, 1024], P('fs', 'tp'), may hold values from -0.125 to 0.125
- key_weight: bfloat16 [2048, 1024], P('fs', 'tp'), may hold values from -0.125 to 0.125
- value_weight: bfloat16 [2048, 2048], P('fs', 'tp'), may hold values from -0.125 to 0.125
- head_gain: float32 [2048], P('tp'), may hold values from 0.1 to 1.9
- out_weight: bfloat16 [2048, 2048], P('tp', 'fs'), may hold values from -0.125 to 0.125
- mlp_gain: float32 [2048], replicated, may hold values from 0.1 to 1.9
- gate_weight: bfloat16 [2048, 2816], P('fs', 'tp'), may hold values from -0.125 to 0.125
- up_weight: bfloat16 [2048, 2816], P('fs', 'tp'), may hold values from -0.125 to 0.125
- down_weight: bfloat16 [2816, 2048], P('tp', 'fs'), may hold values from -0.109375 to 0.109375
Outputs:
- layer_out: bfloat16 [49152, 2048], P(('rep', 'fs', 'tp'))
All inputs are finite; a program needn't handle non-finite values.
Results may differ from a plain program's by a relative error of at most 0.014.
Values may be sent and summed in bfloat16 or wider, within the bound.
A program may use at most 128 MiB of HBM per device.

v0:
```python
import jax
import jax.numpy as jnp
from jax import lax
from jax.sharding import Mesh
from jax.sharding import PartitionSpec as P

DK = 256
DV = 512
BLOCK = 128
FS = ("fs_0", "fs_1", "fs_2")
REP_FS_TP = ("rep", "fs_0", "fs_1", "fs_2", "tp")


norm_eps = 1e-06
rope_base = 10000.0


def cut_along(shard, dim, peers):
    lengths = shard.shape
    pieces = shard.reshape(*lengths[:dim], peers, lengths[dim] // peers, *lengths[dim + 1 :])
    return jnp.moveaxis(pieces, dim, 0)


def sum_at_owner(shard, axis, dim):
    pieces = cut_along(shard, dim, lax.axis_size(axis))
    arrived = lax.all_to_all(pieces, axis, split_axis=0, concat_axis=0, tiled=True)
    return arrived.astype(jnp.float32).sum(axis=0)


def laid_out(pieces, dim):
    pieces = jnp.moveaxis(pieces, 0, dim)
    lengths = pieces.shape
    return pieces.reshape(*lengths[:dim], lengths[dim] * lengths[dim + 1], *lengths[dim + 2 :])


def stacked_from(shard, axes, order):
    pieces = shard
    for k in order:
        pieces = lax.all_gather(pieces, axes[k])
    done = order[::-1]
    back = [done.index(k) for k in range(len(axes))]
    pieces = pieces.transpose(*back, *range(len(axes), pieces.ndim))
    return pieces.reshape(-1, *shard.shape)


def whole_of(shard, axes, order, dim):
    return laid_out(stacked_from(shard, axes, order), dim)


def rms_scale(values, gain):
    widened = values.astype(jnp.float32)
    scaled = widened * lax.rsqrt(jnp.mean(widened * widened, axis=-1, keepdims=True) + norm_eps)
    return (scaled * gain).astype(jnp.bfloat16)


def rotate(vectors):
    length_total = vectors.shape[0]
    half_width = vectors.shape[-1] // 2
    position = jnp.arange(length_total, dtype=jnp.float32)
    inverse = 1.0 / rope_base ** jnp.linspace(0.0, 1.0, half_width, dtype=jnp.float32)
    angle = position[:, None] * inverse[None, :]
    cosine = jnp.cos(angle)[:, None, :]
    sine = jnp.sin(angle)[:, None, :]
    first = vectors[..., :half_width]
    second = vectors[..., half_width:]
    return jnp.concatenate(
        [first * cosine - second * sine, second * cosine + first * sine], axis=-1
    )


def decay_tables(head_ids, block):
    log_gamma = jnp.log1p(-(2.0 ** (-5.0 - 2.0 * head_ids.astype(jnp.float32))))
    offset = jnp.arange(block, dtype=jnp.float32)
    distance = offset[:, None] - offset[None, :]
    inside = jnp.where(
        distance >= 0, jnp.exp(log_gamma[:, None, None] * jnp.maximum(distance, 0.0)), 0.0
    )
    query_decay = jnp.exp(log_gamma[:, None] * (offset + 1.0))
    key_decay = jnp.exp(log_gamma[:, None] * (block - 1.0 - offset))
    block_decay = jnp.exp(log_gamma * block)
    return (inside, query_decay, key_decay, block_decay)


def retain(queries, keys, values, head_ids, block):
    length_total, heads, key_width = queries.shape
    value_width = values.shape[-1]
    count = length_total // block
    inside, query_decay, key_decay, block_decay = decay_tables(head_ids, block)

    def blocks(tensor):
        return tensor.reshape(count, block, heads, tensor.shape[-1]).transpose(0, 2, 1, 3)

    def advance(memory, inputs):
        query_tile_rows, key_tile_rows, value_block = inputs
        attention_scores = jnp.einsum(
            "zvf,zjf->zvj", query_tile_rows, key_tile_rows, preferred_element_type=jnp.float32
        )
        weights = (attention_scores * inside).astype(jnp.bfloat16)
        within = jnp.einsum(
            "hlm,hmv->hlv", weights, value_block, preferred_element_type=jnp.float32
        )
        carried = (
            jnp.einsum(
                "hld,hdv->hlv",
                query_tile_rows,
                memory.astype(jnp.bfloat16),
                preferred_element_type=jnp.float32,
            )
            * query_decay[:, :, None]
        )
        weighted_keys = (key_tile_rows.astype(jnp.float32) * key_decay[:, :, None]).astype(
            jnp.bfloat16
        )
        memory = memory * block_decay[:, None, None] + jnp.einsum(
            "hld,hlv->hdv", weighted_keys, value_block, preferred_element_type=jnp.float32
        )
        return (memory, within + carried)

    start_state = jnp.zeros((heads, key_width, value_width), jnp.float32)
    _, outputs = lax.scan(advance, start_state, (blocks(queries), blocks(keys), blocks(values)))
    return outputs.transpose(0, 2, 1, 3).reshape(length_total, heads, value_width)


def head_scale(retained, gain):
    scaled = retained * lax.rsqrt(jnp.mean(retained * retained, axis=-1, keepdims=True) + norm_eps)
    return (scaled.reshape(retained.shape[0], -1) * gain).astype(jnp.bfloat16)


def shards(
    resid,
    mix_gain,
    query_weight,
    key_weight,
    value_weight,
    head_gain,
    out_weight,
    mlp_gain,
    gate_weight,
    up_weight,
    down_weight,
):
    token_rows = resid.shape[0]
    length_total = token_rows * lax.axis_size("tp")
    key_cols = query_weight.shape[1]
    heads_here = key_cols // DK
    normed = rms_scale(resid, mix_gain)
    mixer_shard = jnp.concatenate([query_weight, key_weight, value_weight], axis=1)
    mixer_full = lax.all_gather(mixer_shard, FS, axis=0, tiled=True)
    projected = jnp.dot(
        lax.all_gather(normed, "tp", axis=0, tiled=True),
        mixer_full,
        preferred_element_type=jnp.float32,
    ).astype(jnp.bfloat16)
    queries = projected[:, :key_cols].astype(jnp.float32).reshape(length_total, heads_here, DK)
    keys = (
        projected[:, key_cols : 2 * key_cols]
        .astype(jnp.float32)
        .reshape(length_total, heads_here, DK)
    )
    values = projected[:, 2 * key_cols :].reshape(length_total, heads_here, DV)
    query_rot = rotate(queries).astype(jnp.bfloat16)
    key_rot = (rotate(keys) * DK ** (-0.5)).astype(jnp.bfloat16)
    head_ids = lax.axis_index("tp") * heads_here + jnp.arange(heads_here, dtype=jnp.int32)
    retained = retain(query_rot, key_rot, values, head_ids, BLOCK)
    head_out = head_scale(retained, head_gain)
    out_full = lax.all_gather(out_weight, FS, axis=1, tiled=True)
    selected = head_out
    mixer_sum = sum_at_owner(
        jnp.dot(selected, out_full, preferred_element_type=jnp.float32).astype(jnp.bfloat16),
        "tp",
        0,
    )
    middle = (resid.astype(jnp.float32) + mixer_sum).astype(jnp.bfloat16)
    normed_mlp = rms_scale(middle, mlp_gain)
    local_units = gate_weight.shape[1]
    mlp_shard = jnp.concatenate([gate_weight, up_weight], axis=1)
    mlp_full = lax.all_gather(mlp_shard, FS, axis=0, tiled=True)
    both = jnp.dot(
        lax.all_gather(normed_mlp, "tp", axis=0, tiled=True),
        mlp_full,
        preferred_element_type=jnp.float32,
    )
    hidden_units = (jax.nn.silu(both[:, :local_units]) * both[:, local_units:]).astype(jnp.bfloat16)
    down_full = whole_of(down_weight, FS, (0, 1, 2), 1)
    selected = hidden_units
    mlp_sum = sum_at_owner(
        jnp.dot(selected, down_full, preferred_element_type=jnp.float32).astype(jnp.bfloat16),
        "tp",
        0,
    )
    return (middle.astype(jnp.float32) + mlp_sum).astype(jnp.bfloat16)


def solution(mesh):
    torus = Mesh(
        mesh.devices.reshape(mesh.shape["rep"], 2, 4, 4, mesh.shape["tp"]),
        ("rep", "fs_0", "fs_1", "fs_2", "tp"),
    )
    return jax.shard_map(
        shards,
        mesh=torus,
        in_specs=(
            P(REP_FS_TP, None),
            P(),
            P(FS, "tp"),
            P(FS, "tp"),
            P(FS, "tp"),
            P("tp"),
            P("tp", FS),
            P(),
            P(FS, "tp"),
            P(FS, "tp"),
            P("tp", FS),
        ),
        out_specs=P(REP_FS_TP, None),
        check_vma=False,
    )
```

profile of v0, /device:TPU:1, one launch (start us, length us, event | category | flops | bytes accessed | tf_op | source)
XLA Modules:
  0.0 678.0 jit_solution(7657517100570402122)
XLA Ops:
  6.5 7.8 %all-gather = bf16[2816,64]{0,1:T(8,128)(2,1)S(1)} all-gather(bf16[1408,64]{0,1:T(8,128)(2,1)} %param.25), channel_id=2, replica_groups=mesh['rep'=2,'fs_0'=2,'fs_1'=4,'fs_2'=4,'tp'=2] {'fs_0'}, dimensions={0}, use_global_device_ids=true | all-gather | bytes 540672 | tf_op jit(solution)/shard_map/all_gather | solution.py:39
  15.2 1.8 fusion.44
  17.0 1.6 fusion.46
  20.3 2.2 fusion.58
  22.5 20.7 %all-gather.21.cloned.1.call-done = bf16[8,1408,64]{1,2,0:T(8,128)(2,1)} async-done(((bf16[2,1408,64]{1,2,0:T(8,128)(2,1)}), bf16[8,1408,64]{1,2,0:T(8,128)(2,1)}) %all-gather.21.cloned.1.call-update) | async-done | bytes 1441808 | tf_op jit(solution)/shard_map/all_gather | solution.py:39
  43.3 17.4 %all-gather.11.cloned.1.call-done = bf16[768,2048]{1,0:T(8,128)(2,1)} async-done(((bf16[384,2048]{1,0:T(8,128)(2,1)}), bf16[768,2048]{1,0:T(8,128)(2,1)}) %all-gather.11.cloned.1.call-update) | async-done | bytes 3145744 | tf_op jit(solution)/shard_map/all_gather | solution.py:150
  60.7 148.5 %all-gather.13.cloned.1.call-done = bf16[2048,2048]{1,0:T(8,128)(2,1)} async-done(((bf16[64,2048]{1,0:T(8,128)(2,1)}), bf16[2048,2048]{1,0:T(8,128)(2,1)}) %all-gather.13.cloned.1.call-update) | async-done | bytes 8388624 | tf_op jit(solution)/shard_map/all_gather | solution.py:148
  209.2 10.0 %convolution_convert_fusion = bf16[768,2048]{1,0:T(8,128)(2,1)S(1)} fusion(bf16[768,2048]{1,0:T(8,128)(2,1)} %all-gather.11.cloned.1.call-done, bf16[2048,2048]{1,0:T(8,128)(2,1)} %all-gather.13.cloned.1.call-done), kind=kOutput, calls=%fused_computation.53 | convolution fusion | flops 6444023808 | bytes 14680064 | tf_op jit(solution)/shard_map/dot_general | solution.py:149
  219.2 2.1 slice_convert_fusion
  221.3 1.3 slice.39
  222.7 3.1 reshape.166
  225.7 3.1 reshape.168
  228.8 3.8 reshape_reshape.3
  232.6 3.0 copy.74
  239.2 30.2 %while.15 = (s32[]{:T(128)}, f32[2,256,512]{2,1,0:T(8,128)S(1)}, f32[6,2,128,512]{3,2,1,0:T(8,128)}, bf16[6,2,128,256]{3,2,0,1:T(8,128)(2,1)}, bf16[6,2,128,512]...) while((s32[]{:T(128)}, f32[2,256,512]{2,1,0:T(8,128)S(1)}, ...), condition=%wide.region_2.4_spmd.clone.clone.clone, body=%wide.region_1.3_spmd.clone.clone.clone.sunk | while | flops 186188304 | bytes 5857972 | solution.py:120
  240.4 2.3 fusion.84
  242.8 1.5 convolution_add_fusion.3
  244.4 1.1 convolution_multiply_fusion.3
  245.5 2.2 fusion.84
  247.8 1.5 convolution_add_fusion.3
  249.4 1.1 convolution_multiply_fusion.3
  250.5 2.2 fusion.84
  252.8 1.5 convolution_add_fusion.3
  255.6 2.3 fusion.84
  257.9 1.5 convolution_add_fusion.3
  259.5 1.1 convolution_multiply_fusion.3
  260.6 2.3 fusion.84
  262.9 1.5 convolution_add_fusion.3
  264.5 1.1 convolution_multiply_fusion.3
  265.7 2.2 fusion.84
  267.9 1.5 convolution_add_fusion.3
  269.5 2.2 multiply_reduce_fusion
  271.8 1.2 mul.286
  273.1 2.4 copy.63
  275.5 2.4 copy.50
  277.9 2.4 copy.62
  280.3 87.4 %all-gather.15.cloned.1.call-done = bf16[1024,2048]{0,1:T(8,128)(2,1)} async-done(((bf16[1024,64]{0,1:T(8,128)(2,1)}), bf16[1024,2048]{0,1:T(8,128)(2,1)}) %all-gather.15.cloned.1.call-update) | async-done | bytes 4194320 | tf_op jit(solution)/shard_map/all_gather | solution.py:166
  367.7 7.5 %convolution_convert_fusion.1 = bf16[768,2048]{1,0:T(8,128)(2,1)S(1)} fusion(bf16[1024,2048]{0,1:T(8,128)(2,1)} %all-gather.15.cloned.1.call-done, f32[768,1024]{1,0:T(8,128)} %bitcast.90, f32[768,1024]{1,0:T(8,128)} %bitcast.89, f32[1024]{0:T(1024)S(1)} %copy-done.13), kind=kOutput, calls=%fused_computation.54 | convolution fusion | flops 3225157632 | bytes 13635584 | tf_op jit(solution)/shard_map/dot_general | solution.py:169
  375.2 27.1 %all_to_all.10 = bf16[2,384,2048]{2,1,0:T(8,128)(2,1)S(1)} all-to-all(bf16[2,384,2048]{2,1,0:T(8,128)(2,1)S(1)} %bitcast.91), channel_id=1, replica_groups=mesh['rep'=2,'fs_0'=2,'fs_1'=4,'fs_2'=4,'tp'=2] {'tp'}, dimensions={0} | all-to-all | bytes 6291456 | tf_op jit(solution)/shard_map/all_to_all | solution.py:26
  403.7 1.6 fusion.50
  406.2 44.7 %all-gather.23.cloned.1.call-done = bf16[16,2,1408,64]{2,3,1,0:T(8,128)(2,1)} async-done(((bf16[4,2,1408,64]{2,3,1,0:T(8,128)(2,1)}), bf16[16,2,1408,64]{2,3,1,0:T(8,128)(2,1)}) %all-gather.23.cloned.1.call-update) | async-done | bytes 5767184 | tf_op jit(solution)/shard_map/all_gather | solution.py:39
  450.9 5.7 copy.53
  456.5 11.9 %all-gather.17.cloned.1.call-done = bf16[768,2048]{1,0:T(8,128)(2,1)} async-done(((bf16[384,2048]{1,0:T(8,128)(2,1)}), bf16[768,2048]{1,0:T(8,128)(2,1)}) %all-gather.17.cloned.1.call-update) | async-done | bytes 3145744 | tf_op jit(solution)/shard_map/all_gather | solution.py:179
  468.4 155.2 %all-gather.19.cloned.1.call-done = bf16[2048,2816]{1,0:T(8,128)(2,1)} async-done(((bf16[64,2816]{1,0:T(8,128)(2,1)}), bf16[2048,2816]{1,0:T(8,128)(2,1)}) %all-gather.19.cloned.1.call-update) | async-done | bytes 11534352 | tf_op jit(solution)/shard_map/all_gather | solution.py:177
  623.6 13.8 %fusion.66 = f32[768,2816]{1,0:T(8,128)S(1)} fusion(bf16[768,2048]{1,0:T(8,128)(2,1)} %all-gather.17.cloned.1.call-done, bf16[2048,2816]{1,0:T(8,128)(2,1)} %all-gather.19.cloned.1.call-done), kind=kOutput, calls=%fused_computation.100 | convolution fusion | flops 8858370048 | bytes 23330816 | tf_op jit(solution)/shard_map/dot_general | solution.py:178
  637.5 5.3 convolution_convert_fusion.2
  642.8 26.0 %all_to_all.11 = bf16[2,384,2048]{2,1,0:T(8,128)(2,1)S(1)} all-to-all(bf16[2,384,2048]{2,1,0:T(8,128)(2,1)S(1)} %bitcast.92), channel_id=1, replica_groups=mesh['rep'=2,'fs_0'=2,'fs_1'=4,'fs_2'=4,'tp'=2] {'tp'}, dimensions={0} | all-to-all | bytes 6291456 | tf_op jit(solution)/shard_map/all_to_all | solution.py:26
  669.5 1.6 fusion.51
  (78 shorter events, 12.1 us)
Async XLA Ops:
  6.5 10.5 %copy-start = (bf16[384,2048]{1,0:T(8,128)(2,1)S(1)}, bf16[384,2048]{1,0:T(8,128)(2,1)}, u32[]{:S(2)}) copy-start(bf16[384,2048]{1,0:T(8,128)(2,1)} %param.15) | copy-start | bytes 4718596
  6.5 10.5 %copy-start.11 = (f32[2048]{0:T(1024)S(1)}, f32[2048]{0:T(1024)}, u32[]{:S(2)}) copy-start(f32[2048]{0:T(1024)} %param.16) | copy-start | bytes 24580
  6.5 36.7 %all-gather.21.cloned.1.call-start = ((), (), s32[]{:S(2)}) async-start(), calls=%async_computation.7 | async-start | bytes 1802240 | tf_op jit(solution)/shard_map/all_gather | solution.py:39
  15.1 3.6 copy-start.8
  15.1 3.6 copy-start.9
  15.1 3.6 copy-start.10
  15.1 45.5 %all-gather.11.cloned.1.call-start = ((), (), s32[]{:S(2)}) async-start(), calls=%async_computation.2 | async-start | bytes 4718592 | tf_op jit(solution)/shard_map/all_gather | solution.py:150
  18.6 190.5 %all-gather.13.cloned.1.call-start = ((), (), s32[]{:S(2)}) async-start(), calls=%async_computation.3 | async-start | bytes 8650752 | tf_op jit(solution)/shard_map/all_gather | solution.py:148
  19.5 348.2 %all-gather.15.cloned.1.call-start = ((), (), s32[]{:S(2)}) async-start(), calls=%async_computation.4 | async-start | bytes 4325376 | tf_op jit(solution)/shard_map/all_gather | solution.py:166
  20.1 430.8 %all-gather.23.cloned.1.call-start = ((), (), s32[]{:S(2)}) async-start(), calls=%async_computation.8 | async-start | bytes 7208960 | tf_op jit(solution)/shard_map/all_gather | solution.py:39
  43.2 425.2 %all-gather.17.cloned.1.call-start = ((), (), s32[]{:S(2)}) async-start(), calls=%async_computation.5 | async-start | bytes 4718592 | tf_op jit(solution)/shard_map/all_gather | solution.py:179
  232.6 3.0 copy-start.2
  232.6 3.0 copy-start.3
  235.6 1.1 copy-start.5
  273.1 2.4 copy-start.1
  277.9 89.8 %copy-start.13 = (f32[1024]{0:T(1024)S(1)}, f32[1024]{0:T(1024)}, u32[]{:S(2)}) copy-start(f32[1024]{0:T(1024)} %param.20) | copy-start | bytes 12292
  403.0 0.7 copy-start.12
  403.6 1.8 copy-start.6
  403.6 1.8 copy-start.7
  405.3 218.3 %all-gather.19.cloned.1.call-start = ((), (), s32[]{:S(2)}) async-start(), calls=%async_computation.6 | async-start | bytes 11894784 | tf_op jit(solution)/shard_map/all_gather | solution.py:177
  623.6 13.8 %copy-start.4 = (bf16[2,4,4,1408,64]{3,4,2,1,0:T(8,128)(2,1)S(1)}, bf16[2,4,4,1408,64]{3,4,2,1,0:T(8,128)(2,1)}, u32[]{:S(2)}) copy-start(bf16[2,4,4,1408,64]{3,4,2,1,0:T(8,128)(2,1)} %copy.53) | copy-start | bytes 17301508
Sparse Core Ops, SparseCore 0:
  15.2 27.9 all-gather.20
  44.9 15.7 all-gather.10
  62.3 146.7 all-gather.12
  210.7 157.0 all-gather.14
  369.2 81.5 all-gather.22
  452.4 15.9 all-gather.16
  470.0 153.5 all-gather.18
where the time goes:
time: 679 us; the launch traced here: 678 us
  waiting for transfers between devices  486 us (72%)
  matrix products  66.2 us (10%)
  blocking collectives  60.8 us (9%)
  local copies, waits for them, and re-layouts  30.7 us (5%)
  other arithmetic  19.8 us (3%)
  between operations  13.8 us (2%)
    all_gather x1, waiting for transfers between devices, shards(): mlp_full = lax.all_gather(mlp_shard, FS, axis=0, tiled=True)  155 us
    all_gather x1, waiting for transfers between devices, shards(): mixer_full = lax.all_gather(mixer_shard, FS, axis=0, tiled=True)  148 us
    all_gather x1, waiting for transfers between devices, shards(): out_full = lax.all_gather(out_weight, FS, axis=1, tiled=True)  87.4 us
    all_gather x2, waiting for transfers between devices, stacked_from(): pieces = lax.all_gather(pieces, axes[k])  65.4 us
    all_to_all x2, blocking collectives, sum_at_owner(): lax.all_to_all(pieces, axis, split_axis=0, concat_axis=0, tiled=True)  53 us
    all_gather x1, waiting for transfers between devices, shards(): lax.all_gather(normed, 'tp', axis=0, tiled=True)  17.4 us
    dot_general x1, matrix products, shards(): jnp.dot(lax.all_gather(normed_mlp, 'tp', axis=0, tiled=True), mlp_full, p...  13.8 us
    dot_general x6, matrix products, advance(): jnp.einsum('hlm,hmv->hlv', weights, value_block, preferred_element_type=j...  13.6 us
  transfers between devices with their start and end apart: 7, of which 7 were waited for; matrix products, arithmetic and copies ran while one was open for 14% of the time, Pallas kernels for 0%

commit v1 on v0

--- a/solution.py
+++ b/solution.py
@@ -1,6 +1,10 @@
+import heapq
+
 import jax
 import jax.numpy as jnp
 from jax import lax
+from jax.experimental import pallas as pl
+from jax.experimental.pallas import tpu as pltpu
 from jax.sharding import Mesh
 from jax.sharding import PartitionSpec as P
 
@@ -9,10 +13,166 @@
 BLOCK = 128
 FS = ("fs_0", "fs_1", "fs_2")
 REP_FS_TP = ("rep", "fs_0", "fs_1", "fs_2", "tp")
-
+MESH_ID = pl.DeviceIdType.MESH
+PIECES = 4
+ROWS = 64
+PIECE_ROWS = ROWS // PIECES
+WIDTHS = (2048, 1024, 2816, 1408)
+OFFSETS = [(z, y, x) for z in range(2) for y in range(4) for x in range(4)]
+ROOT = (0, 0, 0)
 
 norm_eps = 1e-06
 rope_base = 10000.0
+
+
+def parent(piece, offset):
+    z, y, x = offset
+    for axis in ("zxy", "zyx", "xzy", "yzx")[piece]:
+        if axis == "z" and z:
+            return 4 + (x + y + piece) % 2, (0, y, x)
+        if axis == "x" and x:
+            up = x == 1 or (x == 2 and (piece == 1 or (piece in (0, 2) and (y + z + piece // 2) % 2 == 0)))
+            return (0, (z, y, x - 1)) if up else (1, (z, y, (x + 1) % 4))
+        if axis == "y" and y:
+            up = y == 1 or (y == 2 and (piece == 0 or (piece in (1, 3) and (x + z) % 2 == 0)))
+            return (2, (z, y - 1, x)) if up else (3, (z, (y + 1) % 4, x))
+    return None
+
+
+def copy_order(widths, rate=46.6e3, latency=2.2, lead=3.0):
+    kids = {}
+    for piece in range(PIECES):
+        for offset in OFFSETS[1:]:
+            d, above = parent(piece, offset)
+            kids.setdefault((piece, above), []).append((offset, d))
+
+    def depth(piece, offset):
+        return max([0] + [1 + depth(piece, c) for c, _ in kids.get((piece, offset), [])])
+
+    ready = [[] for _ in range(6)]
+    free = [0.0] * 6
+    arrival = {}
+    events = []
+    sends = []
+    for array in range(len(widths)):
+        for piece in range(PIECES):
+            heapq.heappush(events, (0.0, 0, (array, piece, ROOT)))
+    while events:
+        now = events[0][0]
+        while events and events[0][0] <= now + 1e-9:
+            _, kind, item = heapq.heappop(events)
+            if kind == 0:
+                arrival[item] = now
+                array, piece, offset = item
+                for child, d in kids.get((piece, offset), []):
+                    heapq.heappush(ready[d], (array, -depth(piece, child), piece, child, offset))
+        for d in range(6):
+            if free[d] <= now + 1e-9 and ready[d]:
+                array, _, piece, child, offset = heapq.heappop(ready[d])
+                wire = widths[array] * 2 * PIECE_ROWS / rate
+                issue = max(arrival[array, piece, offset], now - lead)
+                sends.append((issue, now, d, array, piece, offset, child))
+                free[d] = now + wire
+                heapq.heappush(events, (now + wire, 1, (0, 0, ROOT)))
+                heapq.heappush(events, (now + wire + latency, 0, (array, piece, child)))
+    sends.sort()
+    return sends, arrival
+
+
+SENDS, ARRIVAL = copy_order(WIDTHS)
+
+
+def slot_of(array, piece, offset):
+    return (array * PIECES + piece) * len(OFFSETS) + OFFSETS.index(offset)
+
+
+def gather_kernel(q_ref, k_ref, v_ref, o_ref, g_ref, u_ref, d_ref, qkv, out, mlp, down, recv, send, local):
+    fulls = (qkv, out, mlp, down)
+    rep, lo, my, mx, core = (lax.axis_index(a) for a in REP_FS_TP)
+    z = rep * 2 + lo
+    zu, zd = lax.rem(z + 1, 4), lax.rem(z + 3, 4)
+    peers = (
+        {"fs_2": lax.rem(mx + 1, 4)},
+        {"fs_2": lax.rem(mx + 3, 4)},
+        {"fs_1": lax.rem(my + 1, 4)},
+        {"fs_1": lax.rem(my + 3, 4)},
+        {"rep": zu // 2, "fs_0": lax.rem(zu, 2)},
+        {"rep": zd // 2, "fs_0": lax.rem(zd, 2)},
+    )
+    barrier = pltpu.get_barrier_semaphore()
+    for peer in peers:
+        pl.semaphore_signal(barrier, inc=1, device_id=peer, device_id_type=MESH_ID)
+
+    def base(offset):
+        oz, oy, ox = offset
+        owner = (lax.rem(lo + oz, 2) * 4 + lax.rem(my + 4 - oy, 4)) * 4 + lax.rem(mx + 4 - ox, 4)
+        return owner * ROWS
+
+    mine = pl.multiple_of(base(ROOT), ROWS)
+    own = pl.ds(mine, ROWS)
+    fills = [
+        (q_ref, qkv.at[own, pl.ds(0, 512)]),
+        (k_ref, qkv.at[own, pl.ds(512, 512)]),
+        (v_ref, qkv.at[own, pl.ds(1024, 1024)]),
+        (o_ref, out.at[own, :]),
+        (g_ref, mlp.at[own, pl.ds(0, 1408)]),
+        (u_ref, mlp.at[own, pl.ds(1408, 1408)]),
+        (d_ref, down.at[own, :]),
+    ]
+    fills = [pltpu.make_async_copy(a, b, local.at[i]) for i, (a, b) in enumerate(fills)]
+    for fill in fills:
+        fill.start()
+    for fill in fills:
+        fill.wait()
+    pl.semaphore_wait(barrier, 6)
+
+    def chunk(array, piece, offset):
+        start = pl.multiple_of(base(offset) + piece * PIECE_ROWS, PIECE_ROWS)
+        return fulls[array].at[pl.ds(start, PIECE_ROWS), :]
+
+    waited = set()
+
+    def arrive(array, piece, offset):
+        if offset == ROOT or (array, piece, offset) in waited:
+            return
+        waited.add((array, piece, offset))
+        here = chunk(array, piece, offset)
+        pltpu.make_async_copy(here, here, recv.at[slot_of(array, piece, offset)]).wait()
+
+    for _, _, d, array, piece, offset, child in SENDS:
+        arrive(array, piece, offset)
+        here = chunk(array, piece, offset)
+        pltpu.make_async_remote_copy(
+            src_ref=here,
+            dst_ref=here,
+            send_sem=send.at[array],
+            recv_sem=recv.at[slot_of(array, piece, child)],
+            device_id=peers[d],
+            device_id_type=MESH_ID,
+        ).start()
+    for array, piece, offset in sorted(ARRIVAL, key=ARRIVAL.get):
+        arrive(array, piece, offset)
+    for array, full in enumerate(fulls):
+        sent = full.at[pl.ds(0, 31 * ROWS), :]
+        pltpu.make_async_copy(sent, sent, send.at[array]).wait()
+
+
+def gather_all(query, key, value, out_t, gate, up, down_t):
+    anywhere = pl.BlockSpec(memory_space=pl.ANY)
+    return pl.pallas_call(
+        gather_kernel,
+        out_shape=[jax.ShapeDtypeStruct((32 * ROWS, w), jnp.bfloat16) for w in WIDTHS],
+        in_specs=[anywhere] * 7,
+        out_specs=[pl.BlockSpec(memory_space=pltpu.VMEM)] * 4,
+        scratch_shapes=[
+            pltpu.SemaphoreType.DMA((4 * PIECES * len(OFFSETS),)),
+            pltpu.SemaphoreType.DMA((4,)),
+            pltpu.SemaphoreType.DMA((7,)),
+        ],
+        compiler_params=pltpu.CompilerParams(
+            collective_id=0, has_side_effects=True, vmem_limit_bytes=56 << 20
+        ),
+    )(query, key, value, out_t, gate, up, down_t)
 
 
 def cut_along(shard, dim, peers):
@@ -25,26 +185,6 @@
     pieces = cut_along(shard, dim, lax.axis_size(axis))
     arrived = lax.all_to_all(pieces, axis, split_axis=0, concat_axis=0, tiled=True)
     return arrived.astype(jnp.float32).sum(axis=0)
-
-
-def laid_out(pieces, dim):
-    pieces = jnp.moveaxis(pieces, 0, dim)
-    lengths = pieces.shape
-    return pieces.reshape(*lengths[:dim], lengths[dim] * lengths[dim + 1], *lengths[dim + 2 :])
-
-
-def stacked_from(shard, axes, order):
-    pieces = shard
-    for k in order:
-        pieces = lax.all_gather(pieces, axes[k])
-    done = order[::-1]
-    back = [done.index(k) for k in range(len(axes))]
-    pieces = pieces.transpose(*back, *range(len(axes), pieces.ndim))
-    return pieces.reshape(-1, *shard.shape)
-
-
-def whole_of(shard, axes, order, dim):
-    return laid_out(stacked_from(shard, axes, order), dim)
 
 
 def rms_scale(values, gain):
@@ -144,8 +284,9 @@
     key_cols = query_weight.shape[1]
     heads_here = key_cols // DK
     normed = rms_scale(resid, mix_gain)
-    mixer_shard = jnp.concatenate([query_weight, key_weight, value_weight], axis=1)
-    mixer_full = lax.all_gather(mixer_shard, FS, axis=0, tiled=True)
+    mixer_full, out_full, mlp_full, down_full = gather_all(
+        query_weight, key_weight, value_weight, out_weight.T, gate_weight, up_weight, down_weight.T
+    )
     projected = jnp.dot(
         lax.all_gather(normed, "tp", axis=0, tiled=True),
         mixer_full,
@@ -163,28 +304,28 @@
     head_ids = lax.axis_index("tp") * heads_here + jnp.arange(heads_here, dtype=jnp.int32)
     retained = retain(query_rot, key_rot, values, head_ids, BLOCK)
     head_out = head_scale(retained, head_gain)
-    out_full = lax.all_gather(out_weight, FS, axis=1, tiled=True)
     selected = head_out
     mixer_sum = sum_at_owner(
-        jnp.dot(selected, out_full, preferred_element_type=jnp.float32).astype(jnp.bfloat16),
+        lax.dot_general(
+            selected, out_full, (((1,), (1,)), ((), ())), preferred_element_type=jnp.float32
+        ).astype(jnp.bfloat16),
         "tp",
         0,
     )
     middle = (resid.astype(jnp.float32) + mixer_sum).astype(jnp.bfloat16)
     normed_mlp = rms_scale(middle, mlp_gain)
     local_units = gate_weight.shape[1]
-    mlp_shard = jnp.concatenate([gate_weight, up_weight], axis=1)
-    mlp_full = lax.all_gather(mlp_shard, FS, axis=0, tiled=True)
     both = jnp.dot(
         lax.all_gather(normed_mlp, "tp", axis=0, tiled=True),
         mlp_full,
         preferred_element_type=jnp.float32,
     )
     hidden_units = (jax.nn.silu(both[:, :local_units]) * both[:, local_units:]).astype(jnp.bfloat16)
-    down_full = whole_of(down_weight, FS, (0, 1, 2), 1)
     selected = hidden_units
     mlp_sum = sum_at_owner(
-        jnp.dot(selected, down_full, preferred_element_type=jnp.float32).astype(jnp.bfloat16),
+        lax.dot_general(
+            selected, down_full, (((1,), (1,)), ((), ())), preferred_element_type=jnp.float32
+        ).astype(jnp.bfloat16),
         "tp",
         0,
     )

time: 679 us -> 275 us (0.41)
  waiting for transfers between devices: 486 us -> 12.3 us
  Pallas kernels: 0 us -> 127 us
  blocking collectives: 60.8 us -> 16.8 us
  local copies, waits for them, and re-layouts: 30.7 us -> 21 us
    all_gather x5 -> x0, waiting for transfers between devices: 456 us -> none  [the longest x1 155 us: shards(): mlp_full = lax.all_gather(mlp_shard, FS, axis=0, tiled=True)]
    pallas_call x0 -> x1, Pallas kernels: none -> 127 us  [gather_all(): pl.pallas_call(gather_kernel, out_shape=[jax.ShapeDtypeStruct((32 * ROWS,...]
    all_to_all x2, blocking collectives: 53 us -> 16.8 us  [sum_at_owner(): lax.all_to_all(pieces, axis, split_axis=0, concat_axis=0, tiled=True)]
    all_gather x1, waiting for transfers between devices: 17.4 us -> 0.01 us  [shards(): lax.all_gather(normed, 'tp', axis=0, tiled=True)]
    all_gather x1 -> x0, blocking collectives: 7.76 us -> none  [stacked_from(): pieces = lax.all_gather(pieces, axes[k])]
  transfers between devices with their start and end apart: 7 -> 2, of which waited for: 7 -> 1; matrix products, arithmetic and copies ran while one was open for 14% -> 1% of each run, Pallas kernels for 0% -> 46%
where the time goes in v1:
time: 275 us; the launch traced here: 274 us
  Pallas kernels  127 us (46%)
  matrix products  63.6 us (23%)
  local copies, waits for them, and re-layouts  21 us (8%)
  other arithmetic  20.2 us (7%)
  blocking collectives  16.8 us (6%)
  between operations  13.6 us (5%)
  waiting for transfers between devices  12.3 us (4%)
    pallas_call x1, Pallas kernels, gather_all(): pl.pallas_call(gather_kernel, out_shape=[jax.ShapeDtypeStruct((32 * ROWS,...  127 us
    all_to_all x2, blocking collectives, sum_at_owner(): lax.all_to_all(pieces, axis, split_axis=0, concat_axis=0, tiled=True)  16.8 us
    dot_general x1, matrix products, shards(): jnp.dot(lax.all_gather(normed_mlp, 'tp', axis=0, tiled=True), mlp_full, p...  13.7 us
    dot_general x6, matrix products, advance(): jnp.einsum('hlm,hmv->hlv', weights, value_block, preferred_element_type=j...  12.9 us
    all_gather x1, waiting for transfers between devices, shards(): lax.all_gather(normed_mlp, 'tp', axis=0, tiled=True)  12.3 us
    dot_general x1, matrix products, shards(): jnp.dot(lax.all_gather(normed, 'tp', axis=0, tiled=True), mixer_full, pre...  10 us
    dot_general x6, matrix products, advance(): jnp.einsum('hld,hlv->hdv', weighted_keys, value_block, preferred_element_...  8.39 us
    dot_general x1, matrix products, shards(): lax.dot_general(selected, down_full, (((1,), (1,)), ((), ())), preferred_...  8.09 us
  transfers between devices with their start and end apart: 2, of which 1 were waited for; matrix products, arithmetic and copies ran while one was open for 1% of the time, Pallas kernels for 46%

profile of v1, /device:TPU:1, one launch (start us, length us, event | category | flops | bytes accessed | tf_op | source)
XLA Modules:
  0.0 274.3 jit_solution(16378434131175986924)
XLA Ops:
  6.5 1.8 fusion.44
  8.3 3.0 %fusion.46 = bf16[384,2048]{1,0:T(8,128)(2,1)} fusion(bf16[384,2048]{1,0:T(8,128)(2,1)} %param.15, f32[2048]{0:T(1024)} %param.16, f32[384]{0:T(512)S(1)} %add_rsqrt_fusion.1), kind=kLoop, calls=%fused_computation.58 | loop fusion | flops 3145728 | bytes 3155456 | tf_op jit(solution)/shard_map/convert_element_type | solution.py:193
  11.4 126.6 %shard_map.109 = (bf16[2048,2048]{1,0:T(8,128)(2,1)}, bf16[2048,1024]{1,0:T(8,128)(2,1)}, bf16[2048,2816]{1,0:T(8,128)(2,1)}, bf16[2048,1408]{1,0:T(8,128)(2,1)}) custom-call(bf16[64,512]{1,0:T(8,128)(2,1)} %q_ref.1, bf16[64,512]{1,0:T(8,128)(2,1)} %k_ref.1, bf16[64,1024]{1,0:T(8,128)(2,1)} %v_ref.1, bf16[64,1024]{1,0:T(8,128)(2,1)} %bitcast.85, ...), custom_call_target="tpu_custom_call" | custom-call | tf_op jit(solution)/shard_map/pallas_call | solution.py:162
  138.2 2.4 fusion.58
  140.7 10.0 %convolution_convert_fusion = bf16[768,2048]{1,0:T(8,128)(2,1)S(1)} fusion(bf16[768,2048]{1,0:T(8,128)(2,1)} %all-gather.3.cloned.1.call-done, bf16[2048,2048]{1,0:T(8,128)(2,1)} %get-tuple-element.62), kind=kOutput, calls=%fused_computation.53 | convolution fusion | flops 6444023808 | bytes 14680064 | tf_op jit(solution)/shard_map/dot_general | solution.py:290
  150.7 2.5 slice_convert_fusion
  153.4 3.2 %reshape.158 = f32[768,2,256]{2,1,0:T(2,128)} reshape(f32[768,512]{1,0:T(8,128)} %get-tuple-element.253) | data formatting | bytes 3145728 | tf_op jit(solution)/shard_map/reshape | solution.py:299
  156.6 3.0 %reshape.160 = f32[768,2,256]{2,1,0:T(2,128)} reshape(f32[768,512]{1,0:T(8,128)} %get-tuple-element.252) | data formatting | bytes 3145728 | tf_op jit(solution)/shard_map/reshape | solution.py:295
  159.6 2.3 reshape_reshape.3
  162.0 1.8 copy.58
  164.3 1.1 fusion.64
  165.9 1.0 maximum_bitcast_fusion
  166.8 1.0 fusion.56
  167.8 28.8 %while.15 = (s32[]{:T(128)}, f32[2,256,512]{2,1,0:T(8,128)S(1)}, f32[6,2,128,512]{3,2,1,0:T(8,128)}, bf16[6,2,128,256]{3,2,0,1:T(8,128)(2,1)}, bf16[6,2,128,512]...) while((s32[]{:T(128)}, f32[2,256,512]{2,1,0:T(8,128)S(1)}, ...), condition=%wide.region_2.4_spmd.clone.clone.clone, body=%wide.region_1.3_spmd.clone.clone.clone.sunk | while | flops 186188304 | bytes 5858980 | solution.py:260
  167.9 1.1 convolution_multiply_fusion.3
  169.1 2.2 fusion.84
  171.2 1.4 convolution_add_fusion.3
  172.7 1.1 convolution_multiply_fusion.3
  173.9 2.1 fusion.84
  176.0 1.4 convolution_add_fusion.3
  177.5 1.1 convolution_multiply_fusion.3
  178.7 2.1 fusion.84
  180.8 1.4 convolution_add_fusion.3
  182.3 1.1 convolution_multiply_fusion.3
  183.5 2.1 fusion.84
  185.6 1.4 convolution_add_fusion.3
  187.1 1.1 convolution_multiply_fusion.3
  188.2 2.1 fusion.84
  190.4 1.4 convolution_add_fusion.3
  191.9 1.1 convolution_multiply_fusion.3
  193.1 2.2 fusion.84
  195.2 1.4 convolution_add_fusion.3
  196.7 2.2 multiply_reduce_fusion
  199.0 1.3 mul.286
  200.3 0.8 copy.48
  201.1 1.1 copy-done.1
  202.2 2.4 copy.38
  204.7 0.8 copy.47
  205.4 1.4 copy-done.8
  206.8 3.7 %convolution_convert_fusion.1 = bf16[768,2048]{1,0:T(8,128)(2,1)S(1)} fusion(bf16[2048,1024]{1,0:T(8,128)(2,1)S(1)} %copy-done.8, f32[768,1024]{1,0:T(8,128)S(1)} %bitcast.77, f32[768,1024]{1,0:T(8,128)S(1)} %bitcast.76, f32[1024]{0:T(1024)S(1)} %copy-done.9), kind=kOutput, calls=%fused_computation.54 | convolution fusion | flops 3225157632 | bytes 13635584 | tf_op jit(solution)/shard_map/dot_general | solution.py:309
  210.5 10.7 %all_to_all.10 = bf16[2,384,2048]{2,1,0:T(8,128)(2,1)S(1)} all-to-all(bf16[2,384,2048]{2,1,0:T(8,128)(2,1)S(1)} %bitcast.78), channel_id=1, replica_groups=mesh['rep'=2,'fs_0'=2,'fs_1'=4,'fs_2'=4,'tp'=2] {'tp'}, dimensions={0} | all-to-all | bytes 6291456 | tf_op jit(solution)/shard_map/all_to_all | solution.py:186
  221.3 0.7 convert_reduce_fusion.1
  223.4 1.6 fusion.50
  225.0 12.3 %all-gather.5.cloned.1.call-done = bf16[768,2048]{1,0:T(8,128)(2,1)} async-done(((bf16[384,2048]{1,0:T(8,128)(2,1)}), bf16[768,2048]{1,0:T(8,128)(2,1)}) %all-gather.5.cloned.1.call-update) | async-done | bytes 3145744 | tf_op jit(solution)/shard_map/all_gather | solution.py:319
  237.3 13.7 %fusion.66 = f32[768,2816]{1,0:T(8,128)S(1)} fusion(bf16[768,2048]{1,0:T(8,128)(2,1)} %all-gather.5.cloned.1.call-done, bf16[2048,2816]{1,0:T(8,128)(2,1)} %get-tuple-element.65), kind=kOutput, calls=%fused_computation.97 | convolution fusion | flops 8858370048 | bytes 23330816 | tf_op jit(solution)/shard_map/dot_general | solution.py:318
  250.9 8.1 %convolution_convert_fusion.2 = bf16[768,2048]{1,0:T(8,128)(2,1)S(1)} fusion(bf16[2048,1408]{1,0:T(8,128)(2,1)} %get-tuple-element.66, f32[768,2816]{1,0:T(8,128)S(1)} %fusion.66), kind=kOutput, calls=%fused_computation.55 | convolution fusion | flops 4437245952 | bytes 17563648 | tf_op jit(solution)/shard_map/dot_general | solution.py:326
  259.0 6.1 %all_to_all.11 = bf16[2,384,2048]{2,1,0:T(8,128)(2,1)S(1)} all-to-all(bf16[2,384,2048]{2,1,0:T(8,128)(2,1)S(1)} %bitcast.79), channel_id=1, replica_groups=mesh['rep'=2,'fs_0'=2,'fs_1'=4,'fs_2'=4,'tp'=2] {'tp'}, dimensions={0} | all-to-all | bytes 6291456 | tf_op jit(solution)/shard_map/all_to_all | solution.py:186
  265.9 1.6 fusion.51
  (52 shorter events, 4.3 us)
Async XLA Ops:
  6.5 134.1 %all-gather.3.cloned.1.call-start = ((), (), s32[]{:S(2)}) async-start(), calls=%async_computation.2 | async-start | bytes 4718592 | tf_op jit(solution)/shard_map/all_gather | solution.py:291
  11.3 225.9 %all-gather.5.cloned.1.call-start = ((), (), s32[]{:S(2)}) async-start(), calls=%async_computation.3 | async-start | bytes 4718592 | tf_op jit(solution)/shard_map/all_gather | solution.py:319
  150.7 2.7 copy-start.2
  153.4 6.3 %slice-start = ((bf16[768,2048]{1,0:T(8,128)(2,1)}), bf16[768,1024]{1,0:T(8,128)(2,1)S(1)}, s32[]{:S(2)}) async-start(bf16[768,2048]{1,0:T(8,128)(2,1)} %copy-done.2), calls=%async_computation.4 | async-start | bytes 3145728 | tf_op jit(solution)/shard_map/slice | solution.py:301
  162.0 1.9 copy-start.3
  162.0 2.4 copy-start.4
  164.3 1.1 copy-start.5
  164.3 1.1 copy-start.6
  200.3 1.9 copy-start.1
  204.6 2.2 copy-start.8
  204.7 2.2 copy-start.9
  221.3 1.4 copy-start
  222.7 0.7 copy-start.7
Sparse Core Ops, SparseCore 0:
  11.5 18.4 all-gather.2
  225.1 12.1 all-gather.4

commit v2 on v0

v2 whole, which is shorter than its diff:
```python
import heapq

import jax
import jax.numpy as jnp
import numpy as np
from jax import lax
from jax.experimental import pallas as pl
from jax.experimental.pallas import tpu as pltpu
from jax.sharding import Mesh
from jax.sharding import PartitionSpec as P

D = 2048
DK = 256
DV = 512
BLOCK = 128
LEN = 768
HALF = LEN // 2
UNITS = 1408
FS = ("fs_0", "fs_1", "fs_2")
REP_FS_TP = ("rep", "fs_0", "fs_1", "fs_2", "tp")
MESH_ID = pl.DeviceIdType.MESH
PIECES = 4
ROWS = 64
PIECE_ROWS = ROWS // PIECES
ARRAYS = ((0, 0, 1024), (0, 1024, 1024), (1, 0, 1024), (2, 0, 1536), (2, 1536, 1280), (3, 0, UNITS))
WIDTHS = tuple(width for _, _, width in ARRAYS)
LAST = len(ARRAYS) - 1
OFFSETS = [(z, y, x) for z in range(2) for y in range(4) for x in range(4)]
GROUPS = [(z, y) for z in range(2) for y in range(4)]
ROOT = (0, 0, 0)
F32 = jnp.float32
BF16 = jnp.bfloat16

norm_eps = 1e-06
rope_base = 10000.0


def parent(piece, offset):
    z, y, x = offset
    for axis in ("zxy", "zyx", "xzy", "yzx")[piece]:
        if axis == "z" and z:
            return 4 + (x + y + piece) % 2, (0, y, x)
        if axis == "x" and x:
            up = x == 1 or (x == 2 and (piece == 1 or (piece in (0, 2) and (y + z + piece // 2) % 2 == 0)))
            return (0, (z, y, x - 1)) if up else (1, (z, y, (x + 1) % 4))
        if axis == "y" and y:
            up = y == 1 or (y == 2 and (piece == 0 or (piece in (1, 3) and (x + z) % 2 == 0)))
            return (2, (z, y - 1, x)) if up else (3, (z, (y + 1) % 4, x))
    return None


def compute_steps():
    steps = [("norm", (0,), (), 2.0), ("norm", (1,), (), 2.0)]
    steps += [("proj", (j,), (0 if j < 4 else 1,), 1.3) for j in range(8)]
    steps += [("ret", (t, h), (), 1.2) for t in range(LEN // BLOCK) for h in range(2)]
    steps += [("out", (1, j), (2,), 0.5) for j in range(8)]
    steps += [("out", (0, j), (), 0.5) for j in range(8)]
    steps += [("mid", (r,), (), 1.0) for r in range(4)]
    steps += [("trade", (), (), 3.0)]
    steps += [("mlp", (j,), (3 if j < 6 else 4,), 1.5) for j in range(11)]
    steps += [("down", (g,), (("g", g),), 1.2) for g in range(8)]
    return steps


def program_order(steps, rate=47.0e3, latency=2.2, lead=8.0, spare=2.5):
    kids = {}
    for piece in range(PIECES):
        for offset in OFFSETS[1:]:
            d, above = parent(piece, offset)
            kids.setdefault((piece, above), []).append((offset, d))

    def depth(piece, offset):
        return max([0] + [1 + depth(piece, c) for c, _ in kids.get((piece, offset), [])])

    def rank(array, piece, child):
        if array == LAST:
            return (array, GROUPS.index(child[:2]), -depth(piece, child))
        return (array, 0, -depth(piece, child))

    def needs(dep):
        if isinstance(dep, tuple):
            return [(LAST, p, o) for p in range(PIECES) for o in OFFSETS if o[:2] == GROUPS[dep[1]]]
        return [(dep, p, o) for p in range(PIECES) for o in OFFSETS]

    ready = [[] for _ in range(6)]
    free = [0.0] * 6
    coming, arrival = [], {}
    for array in range(len(WIDTHS)):
        for piece in range(PIECES):
            heapq.heappush(coming, (2.0, (array, piece, ROOT)))
    left = [PIECES * len(OFFSETS)] * len(WIDTHS)
    order, now, todo = [], 0.0, list(steps)

    def room(d):
        early = ready[d][0][0][0] <= min(a for a in range(len(WIDTHS)) if left[a])
        return lead if early else spare

    while todo or coming or any(ready):
        while coming and coming[0][0] <= now + 1e-9:
            at, item = heapq.heappop(coming)
            arrival[item] = at
            array, piece, offset = item
            left[array] -= 1
            for child, d in kids.get((piece, offset), []):
                heapq.heappush(ready[d], (rank(array, piece, child), piece, child, offset))
        issued = False
        for d in range(6):
            while ready[d] and free[d] - now < room(d):
                (array, *_), piece, child, offset = heapq.heappop(ready[d])
                free[d] = max(free[d], now) + WIDTHS[array] * 2 * PIECE_ROWS / rate
                heapq.heappush(coming, (free[d] + latency, (array, piece, child)))
                order.append(("send", now, (d, array, piece, offset, child)))
                now += 0.03
                issued = True
        if issued:
            continue
        if todo:
            name, args, deps, cost = todo[0]
            wanted = [c for dep in deps for c in needs(dep)]
            if all(c in arrival for c in wanted):
                wanted.sort(key=lambda c: (arrival[c], c))
                order.append((name, now, (args, wanted)))
                now += cost
                todo.pop(0)
                continue
        nexts = [free[d] - room(d) + 1e-3 for d in range(6) if ready[d]]
        if coming:
            nexts.append(coming[0][0])
        now = max(now, min(nexts))
    return order, arrival, now, max(free)


STEPS = compute_steps()
ORDER, ARRIVAL, _, _ = program_order(STEPS)


def tables():
    position = np.arange(LEN, dtype=np.float32)
    inverse = np.float32(1.0) / np.float32(rope_base) ** np.linspace(0.0, 1.0, DK // 2, dtype=np.float32)
    angle = position[:, None] * inverse[None, :]
    log_gamma = np.log1p(-(2.0 ** (-5.0 - 2.0 * np.arange(4))))
    offset = np.arange(BLOCK)
    distance = offset[:, None] - offset[None, :]
    inside = np.where(distance >= 0, np.exp(log_gamma[:, None, None] * np.maximum(distance, 0)), 0.0)
    query_decay = np.exp(log_gamma[:, None] * (offset + 1.0))
    key_decay = np.exp(log_gamma[:, None] * (BLOCK - 1.0 - offset))
    wide = np.ones((1, 1, BLOCK))
    found = (np.cos(angle), np.sin(angle), inside, query_decay[:, :, None] * wide, key_decay[:, :, None] * wide)
    return tuple(jnp.asarray(t.astype(np.float32)) for t in found)


def layer_kernel(
    resid, mix_gain, q_ref, k_ref, v_ref, head_gain, o_ref, mlp_gain, g_ref, u_ref, d_ref,
    cosine, sine, inside, query_decay, key_decay,
    result,
    wq, wo, wm, wd, rows_in, normed, proj, heads, state, hidden, keep, give, take, keep2, give2, take2,
    recv, send, local, swap_send, swap_recv, put,
):
    buffers = (wq, wo, wm, wd)
    rep, lo, my, mx, core = (lax.axis_index(a) for a in REP_FS_TP)
    z = rep * 2 + lo
    zu, zd = lax.rem(z + 1, 4), lax.rem(z + 3, 4)
    peers = (
        {"fs_2": lax.rem(mx + 1, 4)},
        {"fs_2": lax.rem(mx + 3, 4)},
        {"fs_1": lax.rem(my + 1, 4)},
        {"fs_1": lax.rem(my + 3, 4)},
        {"rep": zu // 2, "fs_0": lax.rem(zu, 2)},
        {"rep": zd // 2, "fs_0": lax.rem(zd, 2)},
    )
    partner = {"tp": 1 - core}
    barrier = pltpu.get_barrier_semaphore()
    for peer in peers + (partner,):
        pl.semaphore_signal(barrier, inc=1, device_id=peer, device_id_type=MESH_ID)

    def base(offset):
        oz, oy, ox = offset
        owner = (lax.rem(lo + oz, 2) * 4 + lax.rem(my + 4 - oy, 4)) * 4 + lax.rem(mx + 4 - ox, 4)
        return owner * ROWS

    own = pl.ds(pl.multiple_of(base(ROOT), ROWS), ROWS)
    mine = pl.multiple_of(core * HALF, HALF)
    other = pl.multiple_of(HALF - core * HALF, HALF)
    half = (mine, other)

    def shard(array):
        buffer, first, width = ARRAYS[array]
        return buffers[buffer].at[own, pl.ds(first, width)]

    parts = {
        0: [(q_ref, wq.at[own, pl.ds(0, 512)]), (k_ref, wq.at[own, pl.ds(512, 512)])],
        1: [(v_ref, wq.at[own, pl.ds(1024, 1024)])],
        2: [(o_ref, wo.at[own, :])],
        3: [],
        4: [],
        5: [(d_ref, wd.at[own, :])],
    }
    for j in range(11):
        for which, ref in enumerate((g_ref, u_ref)):
            there = wm.at[own, pl.ds(256 * j + 128 * which, 128)]
            parts[3 if j < 6 else 4].append((ref.at[:, pl.ds(128 * j, 128)], there))
    for array in range(len(ARRAYS)):
        for source, there in parts[array]:
            pltpu.make_async_copy(source, there, local.at[array]).start()
    fill = pltpu.make_async_copy(resid, rows_in.at[pl.ds(mine, HALF), :], local.at[len(ARRAYS)])
    fill.start()
    pl.semaphore_wait(barrier, 7)

    def swap(source, there, slot):
        return pltpu.make_async_remote_copy(
            src_ref=source,
            dst_ref=there,
            send_sem=swap_send.at[slot],
            recv_sem=swap_recv.at[slot],
            device_id=partner,
            device_id_type=MESH_ID,
        )

    swaps = {0: swap(resid, rows_in.at[pl.ds(mine, HALF), :], 0)}
    swaps[0].start()

    def chunk(array, piece, offset):
        buffer, first, width = ARRAYS[array]
        start = pl.multiple_of(base(offset) + piece * PIECE_ROWS, PIECE_ROWS)
        return buffers[buffer].at[pl.ds(start, PIECE_ROWS), pl.ds(first, width)]

    def slot_of(array, piece, offset):
        return (array * PIECES + piece) * len(OFFSETS) + OFFSETS.index(offset)

    waited = set()

    def arrive(array, piece, offset):
        key = (array,) if offset == ROOT else (array, piece, offset)
        if key in waited:
            return
        waited.add(key)
        if offset == ROOT:
            pltpu.make_async_copy(shard(array), shard(array), local.at[array]).wait()
        else:
            here = chunk(array, piece, offset)
            pltpu.make_async_copy(here, here, recv.at[slot_of(array, piece, offset)]).wait()

    def norm_rows(source, gain, start, count):
        def some(i, _):
            rows = pl.ds(pl.multiple_of(start + i * 32, 32), 32)
            wide = source[rows, :].astype(F32)
            scaled = wide * lax.rsqrt(jnp.mean(wide * wide, axis=-1, keepdims=True) + norm_eps)
            normed[rows, :] = (scaled * gain[...]).astype(BF16)

        lax.fori_loop(0, count // 32, some, None)

    def norm(which):
        if which == 0:
            fill.wait()
        else:
            swaps[0].wait()
        norm_rows(rows_in, mix_gain, half[which], HALF)

    def project(j):
        def some(i, _):
            rows = pl.ds(pl.multiple_of(i * HALF, HALF), HALF)
            columns = pl.ds(256 * j, 256)
            found = jnp.dot(normed[rows, :], wq[:, columns], preferred_element_type=F32).astype(BF16)
            if j < 4:
                wide = found.astype(F32)
                first, second = wide[:, :128], wide[:, 128:]
                c, s = cosine[rows, :], sine[rows, :]
                turned = jnp.concatenate([first * c - second * s, second * c + first * s], axis=1)
                if j >= 2:
                    turned = turned * DK**-0.5
                found = turned.astype(BF16)
            proj[rows, columns] = found

        lax.fori_loop(0, 2, some, None)

    def retain(t, h):
        rows = pl.ds(t * BLOCK, BLOCK)
        head = core * 2 + h
        queries = proj[rows, pl.ds(DK * h, DK)]
        keys = proj[rows, pl.ds(2 * DK + DK * h, DK)]
        values = proj[rows, pl.ds(4 * DK + DV * h, DV)]
        decay = query_decay[head]
        scores = lax.dot_general(queries, keys, (((1,), (1,)), ((), ())), preferred_element_type=F32)
        weights = (scores * inside[head]).astype(BF16)
        found = jnp.dot(weights, values, preferred_element_type=F32)
        if t > 0:
            carried = jnp.dot(queries, state[h].astype(BF16), preferred_element_type=F32)
            found = found + carried * jnp.concatenate([decay] * 4, axis=1)
        if t < LEN // BLOCK - 1:
            fade = key_decay[head]
            faded = (keys.astype(F32) * jnp.concatenate([fade] * 2, axis=1)).astype(BF16)
            fresh = lax.dot_general(faded, values, (((0,), (0,)), ((), ())), preferred_element_type=F32)
            if t > 0:
                last = query_decay[head, BLOCK - 1 : BLOCK, :]
                fresh = state[h] * jnp.concatenate([last] * 4, axis=1) + fresh
            state[h] = fresh
        columns = pl.ds(DV * h, DV)
        scaled = found * lax.rsqrt(jnp.mean(found * found, axis=-1, keepdims=True) + norm_eps)
        heads[rows, columns] = (scaled * head_gain[:, columns]).astype(BF16)

    def give_heads(which, j):
        columns = pl.ds(256 * j, 256)
        share = lax.dot_general(
            heads[pl.ds(half[which], HALF), :], wo[columns, :], (((1,), (1,)), ((), ())), preferred_element_type=F32
        ).astype(BF16)
        (give if which else keep)[:, columns] = share
        if (which, j) == (0, 0):
            swaps[1] = swap(give, take, 1)
            swaps[1].start()

    def middle(r):
        if r == 0:
            swaps[1].wait()
        count = HALF // 4

        def some(i, _):
            here = pl.ds(pl.multiple_of(r * count + i * 32, 32), 32)
            rows = pl.ds(pl.multiple_of(mine + r * count + i * 32, 32), 32)
            added = keep[here, :].astype(F32) + take[here, :].astype(F32)
            rows_in[rows, :] = (rows_in[rows, :].astype(F32) + added).astype(BF16)

        lax.fori_loop(0, count // 32, some, None)
        norm_rows(rows_in, mlp_gain, mine + r * count, count)

    def trade():
        rows = pl.ds(mine, HALF)
        swaps[2] = swap(normed.at[rows, :], normed.at[rows, :], 2)
        swaps[2].start()
        swaps[2].wait()

    def expand(j):
        def some(i, _):
            rows = pl.ds(pl.multiple_of(i * HALF, HALF), HALF)
            both = jnp.dot(normed[rows, :], wm[:, pl.ds(256 * j, 256)], preferred_element_type=F32)
            hidden[rows, pl.ds(128 * j, 128)] = (jax.nn.silu(both[:, :128]) * both[:, 128:]).astype(BF16)

        lax.fori_loop(0, 2, some, None)

    blocks = {}

    def contract(g):
        oz, oy = GROUPS[g]
        block = lax.rem(lo + oz, 2) * 4 + lax.rem(my + 4 - oy, 4)
        blocks[g] = block
        columns = wd[pl.ds(pl.multiple_of(block * 256, 256), 256), :]
        for which in (1, 0):
            share = lax.dot_general(
                hidden[pl.ds(half[which], HALF), :], columns, (((1,), (1,)), ((), ())), preferred_element_type=F32
            ).astype(BF16)
            (give2 if which else keep2)[block] = share
        swaps[3 + g] = swap(give2.at[block], take2.at[block], 3 + g)
        swaps[3 + g].start()

    def writing(g):
        place = result.at[:, pl.ds(pl.multiple_of(blocks[g] * 256, 256), 256)]
        return pltpu.make_async_copy(keep2.at[blocks[g]], place, put.at[g])

    def finish(g):
        swaps[3 + g].wait()
        block = blocks[g]

        def some(i, _):
            here = pl.ds(pl.multiple_of(i * 96, 32), 96)
            rows = pl.ds(pl.multiple_of(mine + i * 96, 32), 96)
            columns = pl.ds(pl.multiple_of(block * 256, 256), 256)
            added = keep2[block, here, :].astype(F32) + take2[block, here, :].astype(F32)
            keep2[block, here, :] = (rows_in[rows, columns].astype(F32) + added).astype(BF16)

        lax.fori_loop(0, HALF // 96, some, None)
        writing(g).start()

    def down(g):
        contract(g)
        if g > 0:
            finish(g - 1)

    run = {
        "norm": norm, "proj": project, "ret": retain, "out": give_heads,
        "mid": middle, "trade": trade, "mlp": expand, "down": down,
    }
    for name, _, what in ORDER:
        if name == "send":
            d, array, piece, offset, child = what
            arrive(array, piece, offset)
            here = chunk(array, piece, offset)
            pltpu.make_async_remote_copy(
                src_ref=here,
                dst_ref=here,
                send_sem=send.at[array],
                recv_sem=recv.at[slot_of(array, piece, child)],
                device_id=peers[d],
                device_id_type=MESH_ID,
            ).start()
        else:
            args, wanted = what
            for item in wanted:
                arrive(*item)
            run[name](*args)
    finish(len(GROUPS) - 1)
    for array, (buffer, first, width) in enumerate(ARRAYS):
        sent = buffers[buffer].at[pl.ds(0, 31 * ROWS), pl.ds(first, width)]
        pltpu.make_async_copy(sent, sent, send.at[array]).wait()
    for g in range(len(GROUPS)):
        writing(g).wait()


def shards(
    resid, mix_gain, query_weight, key_weight, value_weight, head_gain, out_weight, mlp_gain,
    gate_weight, up_weight, down_weight,
):
    anywhere = pl.BlockSpec(memory_space=pl.ANY)
    inside = pl.BlockSpec(memory_space=pltpu.VMEM)
    return pl.pallas_call(
        layer_kernel,
        out_shape=jax.ShapeDtypeStruct((HALF, D), BF16),
        in_specs=[anywhere, inside, anywhere, anywhere, anywhere, inside, anywhere, inside, anywhere, anywhere, anywhere]
        + [inside] * 5,
        out_specs=anywhere,
        scratch_shapes=[
            pltpu.VMEM((D, 2048), BF16),
            pltpu.VMEM((D, 1024), BF16),
            pltpu.VMEM((D, 2 * UNITS), BF16),
            pltpu.VMEM((D, UNITS), BF16),
            pltpu.VMEM((LEN, D), BF16),
            pltpu.VMEM((LEN, D), BF16),
            pltpu.VMEM((LEN, 2048), BF16),
            pltpu.VMEM((LEN, 1024), BF16),
            pltpu.VMEM((2, DK, DV), F32),
            pltpu.VMEM((LEN, UNITS), BF16),
        ]
        + [pltpu.VMEM((HALF, D), BF16)] * 3
        + [pltpu.VMEM((8, HALF, 256), BF16)] * 3
        + [
            pltpu.SemaphoreType.DMA((len(ARRAYS) * PIECES * len(OFFSETS),)),
            pltpu.SemaphoreType.DMA((len(ARRAYS),)),
            pltpu.SemaphoreType.DMA((len(ARRAYS) + 1,)),
            pltpu.SemaphoreType.DMA((11,)),
            pltpu.SemaphoreType.DMA((11,)),
            pltpu.SemaphoreType.DMA((8,)),
        ],
        compiler_params=pltpu.CompilerParams(
            collective_id=0, has_side_effects=True, vmem_limit_bytes=67043328
        ),
    )(
        resid, mix_gain.reshape(1, -1), query_weight, key_weight, value_weight, head_gain.reshape(1, -1),
        out_weight.T, mlp_gain.reshape(1, -1), gate_weight, up_weight, down_weight.T, *tables(),
    )


def solution(mesh):
    torus = Mesh(
        mesh.devices.reshape(mesh.shape["rep"], 2, 4, 4, mesh.shape["tp"]),
        ("rep", "fs_0", "fs_1", "fs_2", "tp"),
    )
    return jax.shard_map(
        shards,
        mesh=torus,
        in_specs=(
            P(REP_FS_TP, None),
            P(),
            P(FS, "tp"),
            P(FS, "tp"),
            P(FS, "tp"),
            P("tp"),
            P("tp", FS),
            P(),
            P(FS, "tp"),
            P(FS, "tp"),
            P("tp", FS),
        ),
        out_specs=P(REP_FS_TP, None),
        check_vma=False,
    )
```

time: 679 us -> 137 us (0.20)
  waiting for transfers between devices: 486 us -> 0 us
  Pallas kernels: 0 us -> 134 us
  matrix products: 66.2 us -> 0 us
  blocking collectives: 60.8 us -> 0 us
  local copies, waits for them, and re-layouts: 30.7 us -> 2.73 us
  other arithmetic: 19.8 us -> 0 us
  between operations: 13.8 us -> 0.01 us
    all_gather x7 -> x0, waiting for transfers between devices: 486 us -> none  [the longest x1 155 us: shards(): mlp_full = lax.all_gather(mlp_shard, FS, axis=0, tiled=True)]
    pallas_call x0 -> x1, Pallas kernels: none -> 134 us  [shards(): pl.pallas_call(layer_kernel, out_shape=jax.ShapeDtypeStruct((HALF, D), BF...]
    dot_general x22 -> x0, matrix products: 66.2 us -> none  [the longest x1 13.8 us: shards(): jnp.dot(lax.all_gather(normed_mlp, 'tp', axis=0, tiled=True), mlp_full, p...]
    all_to_all x2 -> x0, blocking collectives: 53 us -> none  [sum_at_owner(): lax.all_to_all(pieces, axis, split_axis=0, concat_axis=0, tiled=True)]
    transpose x2 -> x0, local copies, waits for them, and re-layouts: 8.11 us -> none  [the longest x1 5.68 us: stacked_from(): pieces = pieces.transpose(*back, *range(len(axes), pieces.ndim))]
    all_gather x1 -> x0, blocking collectives: 7.76 us -> none  [stacked_from(): pieces = lax.all_gather(pieces, axes[k])]
    another operation x2 -> x0, local copies, waits for them, and re-layouts: 6.85 us -> none  [blocks(): tensor.reshape(count, block, heads, tensor.shape[-1]).transpose(0, 2, 1, 3)]
  transfers between devices with their start and end apart: 7 -> 0, of which waited for: 7 -> 0; matrix products, arithmetic and copies ran while one was open for 14% -> 0% of each run, Pallas kernels for 0% -> 0%
where the time goes in v2:
time: 137 us
  Pallas kernels  134 us (98%)
  local copies, waits for them, and re-layouts  2.73 us (2%)
    pallas_call x1, Pallas kernels, shards(): pl.pallas_call(layer_kernel, out_shape=jax.ShapeDtypeStruct((HALF, D), BF...  134 us

profile of v2, /device:TPU:1, one launch (start us, length us, event | category | flops | bytes accessed | tf_op | source)
XLA Modules:
  0.0 136.7 jit_solution(837793872001129094)
XLA Ops:
  0.0 134.0 %shard_map.154 = bf16[384,2048]{1,0:T(8,128)(2,1)} custom-call(bf16[384,2048]{1,0:T(8,128)(2,1)} %resid.1, f32[1,2048]{1,0:T(1,128)} %bitcast.7, bf16[64,512]{1,0:T(8,128)(2,1)} %q_ref.1, bf16[64,512]{1,0:T(8,128)(2,1)} %k_ref.1, bf16[64,1024]{1,0:T(8,128)(2,1)} %v_ref.1, f32[1,1024]{1,0:T(1,128)} %bitcast.9, bf16[64,1024]{1,0:T(8,128)(2,1)} %bitcast.6, ...), custom_call_target="tpu_custom_call" | custom-call | tf_op jit(solution)/shard_map/pallas_call | solution.py:413
  134.0 2.7 %copy.18 = bf16[384,2048]{1,0:T(8,128)(2,1)} copy(bf16[384,2048]{1,0:T(8,128)(2,1)} %shard_map.154) | data formatting | bytes 3145728

commit v3 on v2

--- a/solution.py
+++ b/solution.py
@@ -22,11 +22,14 @@
 PIECES = 4
 ROWS = 64
 PIECE_ROWS = ROWS // PIECES
-ARRAYS = ((0, 0, 1024), (0, 1024, 1024), (1, 0, 1024), (2, 0, 1536), (2, 1536, 1280), (3, 0, UNITS))
+SIDE = 640
+TILE = 128
+ARRAYS = ((0, 0, 1024), (0, 1024, 1024), (1, 0, 1024), (2, 0, 2 * SIDE + TILE), (3, 0, SIDE + TILE))
 WIDTHS = tuple(width for _, _, width in ARRAYS)
 LAST = len(ARRAYS) - 1
+SPLIT = (3, 4)
 OFFSETS = [(z, y, x) for z in range(2) for y in range(4) for x in range(4)]
-GROUPS = [(z, y) for z in range(2) for y in range(4)]
+GROUPS = [(z, y) for y in (0, 1, 3, 2) for z in range(2)]
 ROOT = (0, 0, 0)
 F32 = jnp.float32
 BF16 = jnp.bfloat16
@@ -35,8 +38,16 @@
 rope_base = 10000.0
 
 
-def parent(piece, offset):
+def parent(array, piece, offset):
     z, y, x = offset
+    if array in SPLIT:
+        if y == x == 0:
+            return (4 + piece // 2, ROOT) if z else None
+        if y and (piece < 2 or not x):
+            up = y == 1 or (y == 2 and (x % 2 == 0 if piece < 2 else piece == 2))
+            return (2, (z, y - 1, x)) if up else (3, (z, (y + 1) % 4, x))
+        up = x == 1 or (x == 2 and (y % 2 == 0 if piece >= 2 else piece == 0))
+        return (0, (z, y, x - 1)) if up else (1, (z, y, (x + 1) % 4))
     for axis in ("zxy", "zyx", "xzy", "yzx")[piece]:
         if axis == "z" and z:
             return 4 + (x + y + piece) % 2, (0, y, x)
@@ -50,32 +61,37 @@
 
 
 def compute_steps():
-    steps = [("norm", (0,), (), 2.0), ("norm", (1,), (), 2.0)]
-    steps += [("proj", (j,), (0 if j < 4 else 1,), 1.3) for j in range(8)]
-    steps += [("ret", (t, h), (), 1.2) for t in range(LEN // BLOCK) for h in range(2)]
-    steps += [("out", (1, j), (2,), 0.5) for j in range(8)]
-    steps += [("out", (0, j), (), 0.5) for j in range(8)]
-    steps += [("mid", (r,), (), 1.0) for r in range(4)]
-    steps += [("trade", (), (), 3.0)]
-    steps += [("mlp", (j,), (3 if j < 6 else 4,), 1.5) for j in range(11)]
-    steps += [("down", (g,), (("g", g),), 1.2) for g in range(8)]
+    steps = [("prep", (), (), 2.0, None), ("norm", (0,), (), 4.0, None), ("norm", (1,), (), 4.0, None)]
+    steps += [("proj", (j,), (0 if j < 4 else 1,), 1.2, None) for j in range(8)]
+    steps += [("ret", (t, h), (), 0.6, None) for t in range(LEN // BLOCK) for h in range(2)]
+    steps += [("out", (1, j), (2,), 0.6, None) for j in range(8)]
+    steps += [("out", (0, j), (), 0.6, None) for j in range(8)]
+    steps += [("mid", (r,), (), 1.5, None) for r in range(3)]
+    steps += [("trade", (), (), 0.5, None)]
+    steps += [("mlp", (0, i), (3,), 1.6, None) for i in range(2)]
+    steps += [("mlp", (1, i), (), 1.6, None) for i in range(2)]
+    steps += [("pass", (i,), (), 0.3, (("mid", (i,)), 14.0 + 3.0 * i)) for i in range(3)]
+    steps += [("mlp", (2, i), (), 1.6, None) for i in range(2)]
+    steps += [("mlp", (3, i), (), 1.6, None) for i in range(2)]
+    steps += [("down", (g,), (("g", g),), 2.4, None) for g in range(8)]
     return steps
 
 
 def program_order(steps, rate=47.0e3, latency=2.2, lead=8.0, spare=2.5):
     kids = {}
-    for piece in range(PIECES):
-        for offset in OFFSETS[1:]:
-            d, above = parent(piece, offset)
-            kids.setdefault((piece, above), []).append((offset, d))
-
-    def depth(piece, offset):
-        return max([0] + [1 + depth(piece, c) for c, _ in kids.get((piece, offset), [])])
+    for array in range(len(WIDTHS)):
+        for piece in range(PIECES):
+            for offset in OFFSETS[1:]:
+                d, above = parent(array, piece, offset)
+                kids.setdefault((array, piece, above), []).append((offset, d))
+
+    def depth(*at):
+        return max([0] + [1 + depth(*at[:2], c) for c, _ in kids.get(at, [])])
 
     def rank(array, piece, child):
         if array == LAST:
-            return (array, GROUPS.index(child[:2]), -depth(piece, child))
-        return (array, 0, -depth(piece, child))
+            return (array, max(GROUPS.index(child[:2]), 0), -depth(array, piece, child))
+        return (array, 0, -depth(array, piece, child))
 
     def needs(dep):
         if isinstance(dep, tuple):
@@ -87,9 +103,9 @@
     coming, arrival = [], {}
     for array in range(len(WIDTHS)):
         for piece in range(PIECES):
-            heapq.heappush(coming, (2.0, (array, piece, ROOT)))
+            heapq.heappush(coming, (8.0 if array in SPLIT else 2.0, (array, piece, ROOT)))
     left = [PIECES * len(OFFSETS)] * len(WIDTHS)
-    order, now, todo = [], 0.0, list(steps)
+    order, now, todo, done = [], 0.0, list(steps), {}
 
     def room(d):
         early = ready[d][0][0][0] <= min(a for a in range(len(WIDTHS)) if left[a])
@@ -101,7 +117,7 @@
             arrival[item] = at
             array, piece, offset = item
             left[array] -= 1
-            for child, d in kids.get((piece, offset), []):
+            for child, d in kids.get(item, []):
                 heapq.heappush(ready[d], (rank(array, piece, child), piece, child, offset))
         issued = False
         for d in range(6):
@@ -115,17 +131,21 @@
         if issued:
             continue
         if todo:
-            name, args, deps, cost = todo[0]
+            name, args, deps, cost, after = todo[0]
+            start = done[after[0]] + after[1] if after else 0.0
             wanted = [c for dep in deps for c in needs(dep)]
-            if all(c in arrival for c in wanted):
+            if now >= start and all(c in arrival for c in wanted):
                 wanted.sort(key=lambda c: (arrival[c], c))
                 order.append((name, now, (args, wanted)))
                 now += cost
+                done[name, args] = now
                 todo.pop(0)
                 continue
         nexts = [free[d] - room(d) + 1e-3 for d in range(6) if ready[d]]
         if coming:
             nexts.append(coming[0][0])
+        if todo and start > now:
+            nexts.append(start)
         now = max(now, min(nexts))
     return order, arrival, now, max(free)
 
@@ -153,7 +173,8 @@
     resid, mix_gain, q_ref, k_ref, v_ref, head_gain, o_ref, mlp_gain, g_ref, u_ref, d_ref,
     cosine, sine, inside, query_decay, key_decay,
     result,
-    wq, wo, wm, wd, rows_in, normed, proj, heads, state, hidden, keep, give, take, keep2, give2, take2,
+    wq, wo, wm, wd, other_m, other_d, mixed, rows_in, normed, foreign, proj, heads, state, hidden,
+    keep, give, take, keep2, give2, take2, sums, back,
     recv, send, local, swap_send, swap_recv, put,
 ):
     buffers = (wq, wo, wm, wd)
@@ -183,36 +204,51 @@
     other = pl.multiple_of(HALF - core * HALF, HALF)
     half = (mine, other)
 
-    def shard(array):
-        buffer, first, width = ARRAYS[array]
-        return buffers[buffer].at[own, pl.ds(first, width)]
-
+    ze, zb = lax.rem(z + 1 + 2 * core, 4), lax.rem(z + 3 - 2 * core, 4)
+    helper = {"rep": ze // 2, "fs_0": lax.rem(ze, 2)}
+    helped = {"rep": zb // 2, "fs_0": lax.rem(zb, 2)}
+
+    here_m = pl.ds(pl.multiple_of(lo * (SIDE + TILE), TILE), SIDE)
+    here_d = pl.ds(pl.multiple_of((1 - lo) * (SIDE + TILE), TILE), SIDE)
+    tile = pl.ds(SIDE, TILE)
+    left, right = pl.ds(0, SIDE), pl.ds(SIDE + TILE, SIDE)
     parts = {
         0: [(q_ref, wq.at[own, pl.ds(0, 512)]), (k_ref, wq.at[own, pl.ds(512, 512)])],
         1: [(v_ref, wq.at[own, pl.ds(1024, 1024)])],
         2: [(o_ref, wo.at[own, :])],
-        3: [],
-        4: [],
-        5: [(d_ref, wd.at[own, :])],
+        3: [
+            (g_ref.at[:, tile], mixed.at[0]),
+            (u_ref.at[:, tile], mixed.at[1]),
+            (g_ref.at[:, here_m], wm.at[own, left]),
+            (u_ref.at[:, here_m], wm.at[own, right]),
+            (g_ref.at[:, here_d], other_m.at[:, left]),
+            (u_ref.at[:, here_d], other_m.at[:, right]),
+        ],
+        4: [
+            (d_ref.at[:, here_m], wd.at[own, left]),
+            (d_ref.at[:, tile], wd.at[own, tile]),
+            (d_ref.at[:, here_d], other_d.at[:, left]),
+            (d_ref.at[:, tile], other_d.at[:, tile]),
+        ],
     }
-    for j in range(11):
-        for which, ref in enumerate((g_ref, u_ref)):
-            there = wm.at[own, pl.ds(256 * j + 128 * which, 128)]
-            parts[3 if j < 6 else 4].append((ref.at[:, pl.ds(128 * j, 128)], there))
-    for array in range(len(ARRAYS)):
-        for source, there in parts[array]:
-            pltpu.make_async_copy(source, there, local.at[array]).start()
-    fill = pltpu.make_async_copy(resid, rows_in.at[pl.ds(mine, HALF), :], local.at[len(ARRAYS)])
+    fills = {}
+    for array, pairs in parts.items():
+        fills[array] = []
+        for source, there in pairs:
+            at = sum(len(f) for f in fills.values())
+            fills[array].append(pltpu.make_async_copy(source, there, local.at[at]))
+            fills[array][-1].start()
+    fill = pltpu.make_async_copy(resid, rows_in.at[pl.ds(mine, HALF), :], local.at[15])
     fill.start()
     pl.semaphore_wait(barrier, 7)
 
-    def swap(source, there, slot):
+    def swap(source, there, slot, device=partner):
         return pltpu.make_async_remote_copy(
             src_ref=source,
             dst_ref=there,
             send_sem=swap_send.at[slot],
             recv_sem=swap_recv.at[slot],
-            device_id=partner,
+            device_id=device,
             device_id_type=MESH_ID,
         )
 
@@ -235,10 +271,19 @@
             return
         waited.add(key)
         if offset == ROOT:
-            pltpu.make_async_copy(shard(array), shard(array), local.at[array]).wait()
+            for item in fills[array]:
+                item.wait()
         else:
             here = chunk(array, piece, offset)
             pltpu.make_async_copy(here, here, recv.at[slot_of(array, piece, offset)]).wait()
+
+    def prepare():
+        arrive(3, 0, ROOT)
+        lane = lax.broadcasted_iota(jnp.int32, (ROWS, TILE), 1) // (TILE // 2)
+        gate = mixed[0].astype(F32)
+        up = pltpu.roll(mixed[1].astype(F32), TILE // 2, 1)
+        wm[own, tile] = jnp.where(lane == lo, gate, up).astype(BF16)
+        other_m[:, tile] = jnp.where(lane == 1 - lo, gate, up).astype(BF16)
 
     def norm_rows(source, gain, start, count):
         def some(i, _):
@@ -308,33 +353,66 @@
             swaps[1] = swap(give, take, 1)
             swaps[1].start()
 
+    third = HALF // 3
+
+    def lend(r):
+        here = normed.at[pl.ds(pl.multiple_of(mine + r * third, third), third), :]
+        swaps[2 + r] = swap(here, foreign.at[core, pl.ds(r * third, third), :], 2 + r, helper)
+        swaps[5 + r] = swap(here, here, 5 + r)
+        swaps[2 + r].start()
+        swaps[5 + r].start()
+
     def middle(r):
         if r == 0:
             swaps[1].wait()
-        count = HALF // 4
 
         def some(i, _):
-            here = pl.ds(pl.multiple_of(r * count + i * 32, 32), 32)
-            rows = pl.ds(pl.multiple_of(mine + r * count + i * 32, 32), 32)
+            here = pl.ds(pl.multiple_of(r * third + i * 32, 32), 32)
+            rows = pl.ds(pl.multiple_of(mine + r * third + i * 32, 32), 32)
             added = keep[here, :].astype(F32) + take[here, :].astype(F32)
-            rows_in[rows, :] = (rows_in[rows, :].astype(F32) + added).astype(BF16)
-
-        lax.fori_loop(0, count // 32, some, None)
-        norm_rows(rows_in, mlp_gain, mine + r * count, count)
+            found = (rows_in[rows, :].astype(F32) + added).astype(BF16)
+            rows_in[rows, :] = found
+            wide = found.astype(F32)
+            scaled = wide * lax.rsqrt(jnp.mean(wide * wide, axis=-1, keepdims=True) + norm_eps)
+            normed[rows, :] = (scaled * mlp_gain[...]).astype(BF16)
+
+        lax.fori_loop(0, third // 32, some, None)
+        if r > 0:
+            lend(r - 1)
 
     def trade():
-        rows = pl.ds(mine, HALF)
-        swaps[2] = swap(normed.at[rows, :], normed.at[rows, :], 2)
-        swaps[2].start()
-        swaps[2].wait()
-
-    def expand(j):
-        def some(i, _):
-            rows = pl.ds(pl.multiple_of(i * HALF, HALF), HALF)
-            both = jnp.dot(normed[rows, :], wm[:, pl.ds(256 * j, 256)], preferred_element_type=F32)
-            hidden[rows, pl.ds(128 * j, 128)] = (jax.nn.silu(both[:, :128]) * both[:, 128:]).astype(BF16)
-
-        lax.fori_loop(0, 2, some, None)
+        lend(2)
+
+    def forward(i):
+        swaps[2 + i].wait()
+        here = foreign.at[core, pl.ds(i * third, third), :]
+        swaps[8 + i] = swap(here, here, 8 + i)
+        swaps[8 + i].start()
+
+    quarter = HALF // 2
+
+    def expand(part, i):
+        if (part, i) == (1, 0):
+            for r in range(3):
+                swaps[5 + r].wait()
+        if (part, i) == (3, 0):
+            for r in range(3):
+                swaps[8 + r].wait()
+        side = core if part % 2 == 0 else 1 - core
+        if part < 2:
+            source = normed[pl.ds(pl.multiple_of(side * HALF + i * quarter, quarter), quarter), :]
+        else:
+            source = foreign[side, pl.ds(i * quarter, quarter), :]
+        both = jnp.dot(source, wm[...], preferred_element_type=F32)
+        place = 2 * (part // 2) + side
+        rows = pl.ds(i * quarter, quarter)
+        hidden[place, rows, pl.ds(0, SIDE)] = (
+            jax.nn.silu(both[:, :SIDE]) * both[:, SIDE + TILE :]
+        ).astype(BF16)
+        shared = both[:, SIDE : SIDE + TILE]
+        found = jax.nn.silu(shared) * pltpu.roll(shared, TILE // 2, 1)
+        lane = lax.broadcasted_iota(jnp.int32, (quarter, TILE), 1) // (TILE // 2)
+        hidden[place, rows, tile] = jnp.where(lane == lo, found, 0.0).astype(BF16)
 
     blocks = {}
 
@@ -342,49 +420,78 @@
         oz, oy = GROUPS[g]
         block = lax.rem(lo + oz, 2) * 4 + lax.rem(my + 4 - oy, 4)
         blocks[g] = block
-        columns = wd[pl.ds(pl.multiple_of(block * 256, 256), 256), :]
-        for which in (1, 0):
-            share = lax.dot_general(
-                hidden[pl.ds(half[which], HALF), :], columns, (((1,), (1,)), ((), ())), preferred_element_type=F32
-            ).astype(BF16)
-            (give2 if which else keep2)[block] = share
-        swaps[3 + g] = swap(give2.at[block], take2.at[block], 3 + g)
-        swaps[3 + g].start()
+        weights = wd.at[pl.ds(pl.multiple_of(block * 256, 256), 256), :]
+
+        def some(i, _):
+            for kept, side in ((give2, 1 - core), (keep2, core)):
+                kept[block, i] = lax.dot_general(
+                    hidden[2 * i + side], weights[...], (((1,), (1,)), ((), ())), preferred_element_type=F32
+                ).astype(BF16)
+
+        lax.fori_loop(0, 2, some, None)
+        swaps[11 + g] = swap(give2.at[block], take2.at[block], 11 + g)
+        swaps[11 + g].start()
+
+    def add_foreign(g):
+        swaps[11 + g].wait()
+        block = blocks[g]
+
+        def some(i, _):
+            rows = pl.ds(pl.multiple_of(i * 96, 32), 96)
+            added = keep2[block, 1, rows, :].astype(F32) + take2[block, 1, rows, :].astype(F32)
+            sums[block, rows, :] = added.astype(BF16)
+
+        lax.fori_loop(0, HALF // 96, some, None)
+
+    def send_back(g):
+        swaps[19 + g] = swap(sums.at[blocks[g]], back.at[blocks[g]], 19 + g, helped)
+        swaps[19 + g].start()
 
     def writing(g):
         place = result.at[:, pl.ds(pl.multiple_of(blocks[g] * 256, 256), 256)]
-        return pltpu.make_async_copy(keep2.at[blocks[g]], place, put.at[g])
+        return pltpu.make_async_copy(keep2.at[blocks[g], 0], place, put.at[g])
 
     def finish(g):
-        swaps[3 + g].wait()
         block = blocks[g]
+        swaps[19 + g].wait_send()
+        swap(sums.at[block], back.at[block], 19 + (g ^ 1), helped).wait_recv()
 
         def some(i, _):
             here = pl.ds(pl.multiple_of(i * 96, 32), 96)
             rows = pl.ds(pl.multiple_of(mine + i * 96, 32), 96)
             columns = pl.ds(pl.multiple_of(block * 256, 256), 256)
-            added = keep2[block, here, :].astype(F32) + take2[block, here, :].astype(F32)
-            keep2[block, here, :] = (rows_in[rows, columns].astype(F32) + added).astype(BF16)
+            added = keep2[block, 0, here, :].astype(F32) + take2[block, 0, here, :].astype(F32)
+            added = added + back[block, here, :].astype(F32)
+            keep2[block, 0, here, :] = (rows_in[rows, columns].astype(F32) + added).astype(BF16)
 
         lax.fori_loop(0, HALF // 96, some, None)
         writing(g).start()
 
+    def after_down(g):
+        if 0 <= g - 1 < len(GROUPS):
+            add_foreign(g - 1)
+        if 0 <= g - 4 < len(GROUPS):
+            finish(g - 4)
+        if 0 <= g - 1 < len(GROUPS):
+            send_back(g - 1)
+
     def down(g):
         contract(g)
-        if g > 0:
-            finish(g - 1)
+        after_down(g)
 
     run = {
-        "norm": norm, "proj": project, "ret": retain, "out": give_heads,
-        "mid": middle, "trade": trade, "mlp": expand, "down": down,
+        "prep": prepare, "norm": norm, "proj": project, "ret": retain, "out": give_heads,
+        "mid": middle, "trade": trade, "pass": forward, "mlp": expand, "down": down,
     }
     for name, _, what in ORDER:
         if name == "send":
             d, array, piece, offset, child = what
             arrive(array, piece, offset)
-            here = chunk(array, piece, offset)
+            source = here = chunk(array, piece, offset)
+            if array in SPLIT and child == (1, 0, 0):
+                source = (other_m, other_d)[array - 3].at[pl.ds(piece * PIECE_ROWS, PIECE_ROWS), :]
             pltpu.make_async_remote_copy(
-                src_ref=here,
+                src_ref=source,
                 dst_ref=here,
                 send_sem=send.at[array],
                 recv_sem=recv.at[slot_of(array, piece, child)],
@@ -396,7 +503,8 @@
             for item in wanted:
                 arrive(*item)
             run[name](*args)
-    finish(len(GROUPS) - 1)
+    for g in range(len(GROUPS), len(GROUPS) + 4):
+        after_down(g)
     for array, (buffer, first, width) in enumerate(ARRAYS):
         sent = buffers[buffer].at[pl.ds(0, 31 * ROWS), pl.ds(first, width)]
         pltpu.make_async_copy(sent, sent, send.at[array]).wait()
@@ -419,23 +527,28 @@
         scratch_shapes=[
             pltpu.VMEM((D, 2048), BF16),
             pltpu.VMEM((D, 1024), BF16),
-            pltpu.VMEM((D, 2 * UNITS), BF16),
-            pltpu.VMEM((D, UNITS), BF16),
+            pltpu.VMEM((D, ARRAYS[3][2]), BF16),
+            pltpu.VMEM((D, ARRAYS[4][2]), BF16),
+            pltpu.VMEM((ROWS, ARRAYS[3][2]), BF16),
+            pltpu.VMEM((ROWS, ARRAYS[4][2]), BF16),
+            pltpu.VMEM((2, ROWS, TILE), BF16),
             pltpu.VMEM((LEN, D), BF16),
             pltpu.VMEM((LEN, D), BF16),
+            pltpu.VMEM((2, HALF, D), BF16),
             pltpu.VMEM((LEN, 2048), BF16),
             pltpu.VMEM((LEN, 1024), BF16),
             pltpu.VMEM((2, DK, DV), F32),
-            pltpu.VMEM((LEN, UNITS), BF16),
+            pltpu.VMEM((4, HALF, SIDE + TILE), BF16),
         ]
         + [pltpu.VMEM((HALF, D), BF16)] * 3
-        + [pltpu.VMEM((8, HALF, 256), BF16)] * 3
+        + [pltpu.VMEM((8, 2, HALF, 256), BF16)] * 3
+        + [pltpu.VMEM((8, HALF, 256), BF16)] * 2
         + [
             pltpu.SemaphoreType.DMA((len(ARRAYS) * PIECES * len(OFFSETS),)),
             pltpu.SemaphoreType.DMA((len(ARRAYS),)),
-            pltpu.SemaphoreType.DMA((len(ARRAYS) + 1,)),
-            pltpu.SemaphoreType.DMA((11,)),
-            pltpu.SemaphoreType.DMA((11,)),
+            pltpu.SemaphoreType.DMA((16,)),
+            pltpu.SemaphoreType.DMA((27,)),
+            pltpu.SemaphoreType.DMA((27,)),
             pltpu.SemaphoreType.DMA((8,)),
         ],
         compiler_params=pltpu.CompilerParams(

time: 137 us -> 139 us (1.015)
  no operation moved by 1% of the time
where the time goes in v3:
time: 139 us; the launch traced here: 138 us
  Pallas kernels  135 us (97%)
  local copies, waits for them, and re-layouts  2.73 us (2%)
    pallas_call x1, Pallas kernels, shards(): pl.pallas_call(layer_kernel, out_shape=jax.ShapeDtypeStruct((HALF, D), BF...  135 us

profile of v3, /device:TPU:1, one launch (start us, length us, event | category | flops | bytes accessed | tf_op | source)
XLA Modules:
  0.0 137.9 jit_solution(12706494803695376850)
XLA Ops:
  0.0 135.2 %shard_map.154 = bf16[384,2048]{1,0:T(8,128)(2,1)} custom-call(bf16[384,2048]{1,0:T(8,128)(2,1)} %resid.1, f32[1,2048]{1,0:T(1,128)} %bitcast.7, bf16[64,512]{1,0:T(8,128)(2,1)} %q_ref.1, bf16[64,512]{1,0:T(8,128)(2,1)} %k_ref.1, bf16[64,1024]{1,0:T(8,128)(2,1)} %v_ref.1, f32[1,1024]{1,0:T(1,128)} %bitcast.9, bf16[64,1024]{1,0:T(8,128)(2,1)} %bitcast.6, ...), custom_call_target="tpu_custom_call" | custom-call | tf_op jit(solution)/shard_map/pallas_call | solution.py:521
  135.2 2.7 %copy.18 = bf16[384,2048]{1,0:T(8,128)(2,1)} copy(bf16[384,2048]{1,0:T(8,128)(2,1)} %shard_map.154) | data formatting | bytes 3145728

commit v4 on v3

--- a/solution.py
+++ b/solution.py
@@ -28,6 +28,9 @@
 WIDTHS = tuple(width for _, _, width in ARRAYS)
 LAST = len(ARRAYS) - 1
 SPLIT = (3, 4)
+DUE = (20, 25, 30, 78, 86)
+HOP = 4.0
+LEAD = 4.0
 OFFSETS = [(z, y, x) for z in range(2) for y in range(4) for x in range(4)]
 GROUPS = [(z, y) for y in (0, 1, 3, 2) for z in range(2)]
 ROOT = (0, 0, 0)
@@ -64,20 +67,19 @@
     steps = [("prep", (), (), 2.0, None), ("norm", (0,), (), 4.0, None), ("norm", (1,), (), 4.0, None)]
     steps += [("proj", (j,), (0 if j < 4 else 1,), 1.2, None) for j in range(8)]
     steps += [("ret", (t, h), (), 0.6, None) for t in range(LEN // BLOCK) for h in range(2)]
-    steps += [("out", (1, j), (2,), 0.6, None) for j in range(8)]
-    steps += [("out", (0, j), (), 0.6, None) for j in range(8)]
-    steps += [("mid", (r,), (), 1.5, None) for r in range(3)]
-    steps += [("trade", (), (), 0.5, None)]
-    steps += [("mlp", (0, i), (3,), 1.6, None) for i in range(2)]
-    steps += [("mlp", (1, i), (), 1.6, None) for i in range(2)]
-    steps += [("pass", (i,), (), 0.3, (("mid", (i,)), 14.0 + 3.0 * i)) for i in range(3)]
-    steps += [("mlp", (2, i), (), 1.6, None) for i in range(2)]
+    for r in range(3):
+        steps += [("out", (1, r), (2,), 1.2, None), ("out", (0, r), (), 1.2, None), ("mid", (r,), (), 1.0, None)]
+    steps += [("pass", (i,), (), 0.1, (("mid", (i,)), 8.5 + 3.0 * i)) for i in range(3)]
+    steps += [("mlp", (2, i), (3,), 1.6, None) for i in range(2)]
     steps += [("mlp", (3, i), (), 1.6, None) for i in range(2)]
-    steps += [("down", (g,), (("g", g),), 2.4, None) for g in range(8)]
-    return steps
-
-
-def program_order(steps, rate=47.0e3, latency=2.2, lead=8.0, spare=2.5):
+    tail = [("mlp", (0, i), (), 1.6, None) for i in range(2)] + [("mlp", (1, i), (), 1.6, None) for i in range(2)]
+    tail += [("own", (g,), (), 1.0, None) for g in range(8)]
+    for g in range(8):
+        steps += [("lent", (g,), (("g", g),), 1.2, None)] + (tail[g // 2 : g // 2 + 1] if g % 2 else [])
+    return steps + tail[4:]
+
+
+def program_order(steps, rate=47.0e3, latency=2.2, lead=LEAD):
     kids = {}
     for array in range(len(WIDTHS)):
         for piece in range(PIECES):
@@ -88,10 +90,9 @@
     def depth(*at):
         return max([0] + [1 + depth(*at[:2], c) for c, _ in kids.get(at, [])])
 
-    def rank(array, piece, child):
-        if array == LAST:
-            return (array, max(GROUPS.index(child[:2]), 0), -depth(array, piece, child))
-        return (array, 0, -depth(array, piece, child))
+    def due(array, piece, child):
+        late = GROUPS.index(child[:2]) if array == LAST else 0
+        return DUE[array] + late - HOP * depth(array, piece, child)
 
     def needs(dep):
         if isinstance(dep, tuple):
@@ -104,25 +105,19 @@
     for array in range(len(WIDTHS)):
         for piece in range(PIECES):
             heapq.heappush(coming, (8.0 if array in SPLIT else 2.0, (array, piece, ROOT)))
-    left = [PIECES * len(OFFSETS)] * len(WIDTHS)
     order, now, todo, done = [], 0.0, list(steps), {}
-
-    def room(d):
-        early = ready[d][0][0][0] <= min(a for a in range(len(WIDTHS)) if left[a])
-        return lead if early else spare
 
     while todo or coming or any(ready):
         while coming and coming[0][0] <= now + 1e-9:
             at, item = heapq.heappop(coming)
             arrival[item] = at
             array, piece, offset = item
-            left[array] -= 1
             for child, d in kids.get(item, []):
-                heapq.heappush(ready[d], (rank(array, piece, child), piece, child, offset))
+                heapq.heappush(ready[d], (due(array, piece, child), array, piece, child, offset))
         issued = False
         for d in range(6):
-            while ready[d] and free[d] - now < room(d):
-                (array, *_), piece, child, offset = heapq.heappop(ready[d])
+            while ready[d] and free[d] - now < lead:
+                _, array, piece, child, offset = heapq.heappop(ready[d])
                 free[d] = max(free[d], now) + WIDTHS[array] * 2 * PIECE_ROWS / rate
                 heapq.heappush(coming, (free[d] + latency, (array, piece, child)))
                 order.append(("send", now, (d, array, piece, offset, child)))
@@ -141,7 +136,7 @@
                 done[name, args] = now
                 todo.pop(0)
                 continue
-        nexts = [free[d] - room(d) + 1e-3 for d in range(6) if ready[d]]
+        nexts = [free[d] - lead + 1e-3 for d in range(6) if ready[d]]
         if coming:
             nexts.append(coming[0][0])
         if todo and start > now:
@@ -174,7 +169,7 @@
     cosine, sine, inside, query_decay, key_decay,
     result,
     wq, wo, wm, wd, other_m, other_d, mixed, rows_in, normed, foreign, proj, heads, state, hidden,
-    keep, give, take, keep2, give2, take2, sums, back,
+    keep, give, take, both2, take2, sums, back,
     recv, send, local, swap_send, swap_recv, put,
 ):
     buffers = (wq, wo, wm, wd)
@@ -343,17 +338,23 @@
         scaled = found * lax.rsqrt(jnp.mean(found * found, axis=-1, keepdims=True) + norm_eps)
         heads[rows, columns] = (scaled * head_gain[:, columns]).astype(BF16)
 
-    def give_heads(which, j):
-        columns = pl.ds(256 * j, 256)
-        share = lax.dot_general(
-            heads[pl.ds(half[which], HALF), :], wo[columns, :], (((1,), (1,)), ((), ())), preferred_element_type=F32
-        ).astype(BF16)
-        (give if which else keep)[:, columns] = share
-        if (which, j) == (0, 0):
-            swaps[1] = swap(give, take, 1)
-            swaps[1].start()
-
     third = HALF // 3
+
+    def give_heads(which, r):
+        rows = pl.ds(pl.multiple_of(half[which] + r * third, third), third)
+        there = pl.ds(r * third, third)
+        share = give if which else keep
+
+        def some(j, _):
+            columns = pl.ds(pl.multiple_of(j * 512, 512), 512)
+            share[there, columns] = lax.dot_general(
+                heads[rows, :], wo[columns, :], (((1,), (1,)), ((), ())), preferred_element_type=F32
+            ).astype(BF16)
+
+        lax.fori_loop(0, 4, some, None)
+        if which:
+            swaps[35 + r] = swap(give.at[there, :], take.at[there, :], 35 + r)
+            swaps[35 + r].start()
 
     def lend(r):
         here = normed.at[pl.ds(pl.multiple_of(mine + r * third, third), third), :]
@@ -363,8 +364,7 @@
         swaps[5 + r].start()
 
     def middle(r):
-        if r == 0:
-            swaps[1].wait()
+        swaps[35 + r].wait()
 
         def some(i, _):
             here = pl.ds(pl.multiple_of(r * third + i * 32, 32), 32)
@@ -377,11 +377,7 @@
             normed[rows, :] = (scaled * mlp_gain[...]).astype(BF16)
 
         lax.fori_loop(0, third // 32, some, None)
-        if r > 0:
-            lend(r - 1)
-
-    def trade():
-        lend(2)
+        lend(r)
 
     def forward(i):
         swaps[2 + i].wait()
@@ -413,46 +409,62 @@
         found = jax.nn.silu(shared) * pltpu.roll(shared, TILE // 2, 1)
         lane = lax.broadcasted_iota(jnp.int32, (quarter, TILE), 1) // (TILE // 2)
         hidden[place, rows, tile] = jnp.where(lane == lo, found, 0.0).astype(BF16)
+        if part < 2:
+            send_back()
 
     blocks = {}
 
-    def contract(g):
+    def down_into(g, part, slot):
+        block = blocks[g]
+        weights = wd.at[pl.ds(pl.multiple_of(block * 256, 256), 256), :]
+
+        def some(i, _):
+            side = i * core + (1 - i) * (1 - core)
+            both2[block, part, i] = lax.dot_general(
+                hidden[2 * part + side], weights[...], (((1,), (1,)), ((), ())), preferred_element_type=F32
+            ).astype(BF16)
+
+        lax.fori_loop(0, 2, some, None)
+        swaps[slot] = swap(both2.at[block, part, 0], take2.at[block, part], slot)
+        swaps[slot].start()
+
+    pending = []
+
+    def send_back():
+        for g in pending:
+            swaps[11 + g].wait()
+            block = blocks[g]
+
+            def some(i, _, block=block):
+                rows = pl.ds(pl.multiple_of(i * 96, 32), 96)
+                added = both2[block, 1, 1, rows, :].astype(F32) + take2[block, 1, rows, :].astype(F32)
+                sums[block, rows, :] = added.astype(BF16)
+
+            lax.fori_loop(0, HALF // 96, some, None)
+            swaps[19 + g] = swap(sums.at[block], back.at[block], 19 + g, helped)
+            swaps[19 + g].start()
+        pending.clear()
+
+    def lent(g):
         oz, oy = GROUPS[g]
-        block = lax.rem(lo + oz, 2) * 4 + lax.rem(my + 4 - oy, 4)
-        blocks[g] = block
-        weights = wd.at[pl.ds(pl.multiple_of(block * 256, 256), 256), :]
-
-        def some(i, _):
-            for kept, side in ((give2, 1 - core), (keep2, core)):
-                kept[block, i] = lax.dot_general(
-                    hidden[2 * i + side], weights[...], (((1,), (1,)), ((), ())), preferred_element_type=F32
-                ).astype(BF16)
-
-        lax.fori_loop(0, 2, some, None)
-        swaps[11 + g] = swap(give2.at[block], take2.at[block], 11 + g)
-        swaps[11 + g].start()
-
-    def add_foreign(g):
-        swaps[11 + g].wait()
-        block = blocks[g]
-
-        def some(i, _):
-            rows = pl.ds(pl.multiple_of(i * 96, 32), 96)
-            added = keep2[block, 1, rows, :].astype(F32) + take2[block, 1, rows, :].astype(F32)
-            sums[block, rows, :] = added.astype(BF16)
-
-        lax.fori_loop(0, HALF // 96, some, None)
-
-    def send_back(g):
-        swaps[19 + g] = swap(sums.at[blocks[g]], back.at[blocks[g]], 19 + g, helped)
-        swaps[19 + g].start()
+        blocks[g] = lax.rem(lo + oz, 2) * 4 + lax.rem(my + 4 - oy, 4)
+        down_into(g, 1, 11 + g)
+        send_back()
+        pending.append(g)
+
+    def own_rows(g):
+        down_into(g, 0, 27 + g)
+        send_back()
+        if g >= 2:
+            finish(g - 2)
 
     def writing(g):
         place = result.at[:, pl.ds(pl.multiple_of(blocks[g] * 256, 256), 256)]
-        return pltpu.make_async_copy(keep2.at[blocks[g], 0], place, put.at[g])
+        return pltpu.make_async_copy(both2.at[blocks[g], 0, 1], place, put.at[g])
 
     def finish(g):
         block = blocks[g]
+        swaps[27 + g].wait()
         swaps[19 + g].wait_send()
         swap(sums.at[block], back.at[block], 19 + (g ^ 1), helped).wait_recv()
 
@@ -460,28 +472,16 @@
             here = pl.ds(pl.multiple_of(i * 96, 32), 96)
             rows = pl.ds(pl.multiple_of(mine + i * 96, 32), 96)
             columns = pl.ds(pl.multiple_of(block * 256, 256), 256)
-            added = keep2[block, 0, here, :].astype(F32) + take2[block, 0, here, :].astype(F32)
+            added = both2[block, 0, 1, here, :].astype(F32) + take2[block, 0, here, :].astype(F32)
             added = added + back[block, here, :].astype(F32)
-            keep2[block, 0, here, :] = (rows_in[rows, columns].astype(F32) + added).astype(BF16)
+            both2[block, 0, 1, here, :] = (rows_in[rows, columns].astype(F32) + added).astype(BF16)
 
         lax.fori_loop(0, HALF // 96, some, None)
         writing(g).start()
 
-    def after_down(g):
-        if 0 <= g - 1 < len(GROUPS):
-            add_foreign(g - 1)
-        if 0 <= g - 4 < len(GROUPS):
-            finish(g - 4)
-        if 0 <= g - 1 < len(GROUPS):
-            send_back(g - 1)
-
-    def down(g):
-        contract(g)
-        after_down(g)
-
     run = {
         "prep": prepare, "norm": norm, "proj": project, "ret": retain, "out": give_heads,
-        "mid": middle, "trade": trade, "pass": forward, "mlp": expand, "down": down,
+        "mid": middle, "pass": forward, "mlp": expand, "lent": lent, "own": own_rows,
     }
     for name, _, what in ORDER:
         if name == "send":
@@ -503,8 +503,9 @@
             for item in wanted:
                 arrive(*item)
             run[name](*args)
-    for g in range(len(GROUPS), len(GROUPS) + 4):
-        after_down(g)
+    send_back()
+    finish(len(GROUPS) - 2)
+    finish(len(GROUPS) - 1)
     for array, (buffer, first, width) in enumerate(ARRAYS):
         sent = buffers[buffer].at[pl.ds(0, 31 * ROWS), pl.ds(first, width)]
         pltpu.make_async_copy(sent, sent, send.at[array]).wait()
@@ -541,14 +542,14 @@
             pltpu.VMEM((4, HALF, SIDE + TILE), BF16),
         ]
         + [pltpu.VMEM((HALF, D), BF16)] * 3
-        + [pltpu.VMEM((8, 2, HALF, 256), BF16)] * 3
+        + [pltpu.VMEM((8, 2, 2, HALF, 256), BF16), pltpu.VMEM((8, 2, HALF, 256), BF16)]
         + [pltpu.VMEM((8, HALF, 256), BF16)] * 2
         + [
             pltpu.SemaphoreType.DMA((len(ARRAYS) * PIECES * len(OFFSETS),)),
             pltpu.SemaphoreType.DMA((len(ARRAYS),)),
             pltpu.SemaphoreType.DMA((16,)),
-            pltpu.SemaphoreType.DMA((27,)),
-            pltpu.SemaphoreType.DMA((27,)),
+            pltpu.SemaphoreType.DMA((38,)),
+            pltpu.SemaphoreType.DMA((38,)),
             pltpu.SemaphoreType.DMA((8,)),
         ],
         compiler_params=pltpu.CompilerParams(

time: 139 us -> 129 us (0.928)
  Pallas kernels: 135 us -> 126 us
    pallas_call x1, Pallas kernels: 135 us -> 126 us  [shards(): pl.pallas_call(layer_kernel, out_shape=jax.ShapeDtypeStruct((HALF, D), BF...]
where the time goes in v4:
time: 129 us; the launch traced here: 128 us
  Pallas kernels  126 us (98%)
  local copies, waits for them, and re-layouts  2.73 us (2%)
    pallas_call x1, Pallas kernels, shards(): pl.pallas_call(layer_kernel, out_shape=jax.ShapeDtypeStruct((HALF, D), BF...  126 us
    unnamed x1, local copies, waits for them, and re-layouts  2.73 us

profile of v4, /device:TPU:1, one launch (start us, length us, event | category | flops | bytes accessed | tf_op | source)
XLA Modules:
  0.0 128.4 jit_solution(8924200244128093006)
XLA Ops:
  0.0 125.6 %shard_map.154 = bf16[384,2048]{1,0:T(8,128)(2,1)} custom-call(bf16[384,2048]{1,0:T(8,128)(2,1)} %resid.1, f32[1,2048]{1,0:T(1,128)} %bitcast.7, bf16[64,512]{1,0:T(8,128)(2,1)} %q_ref.1, bf16[64,512]{1,0:T(8,128)(2,1)} %k_ref.1, bf16[64,1024]{1,0:T(8,128)(2,1)} %v_ref.1, f32[1,1024]{1,0:T(1,128)} %bitcast.9, bf16[64,1024]{1,0:T(8,128)(2,1)} %bitcast.6, ...), custom_call_target="tpu_custom_call" | custom-call | tf_op jit(solution)/shard_map/pallas_call | solution.py:522
  125.6 2.7 %copy.18 = bf16[384,2048]{1,0:T(8,128)(2,1)} copy(bf16[384,2048]{1,0:T(8,128)(2,1)} %shard_map.154) | data formatting | bytes 3145728

commit v5 on v4

--- a/solution.py
+++ b/solution.py
@@ -19,16 +19,16 @@
 FS = ("fs_0", "fs_1", "fs_2")
 REP_FS_TP = ("rep", "fs_0", "fs_1", "fs_2", "tp")
 MESH_ID = pl.DeviceIdType.MESH
-PIECES = 4
 ROWS = 64
-PIECE_ROWS = ROWS // PIECES
 SIDE = 640
 TILE = 128
-ARRAYS = ((0, 0, 1024), (0, 1024, 1024), (1, 0, 1024), (2, 0, 2 * SIDE + TILE), (3, 0, SIDE + TILE))
+FIRST = 384
+ARRAYS = ((0, 0, 1024), (0, 1024, 1024), (1, 0, 1024), (2, 0, 2 * FIRST), (2, 2 * FIRST, 640), (3, 0, SIDE + TILE))
+PIECES = (4, 4, 4, 2, 2, 2)
 WIDTHS = tuple(width for _, _, width in ARRAYS)
 LAST = len(ARRAYS) - 1
-SPLIT = (3, 4)
-DUE = (20, 25, 30, 78, 86)
+SPLIT = (3, 4, 5)
+DUE = (20, 25, 30, 66, 78, 86)
 HOP = 4.0
 LEAD = 4.0
 OFFSETS = [(z, y, x) for z in range(2) for y in range(4) for x in range(4)]
@@ -45,11 +45,11 @@
     z, y, x = offset
     if array in SPLIT:
         if y == x == 0:
-            return (4 + piece // 2, ROOT) if z else None
-        if y and (piece < 2 or not x):
-            up = y == 1 or (y == 2 and (x % 2 == 0 if piece < 2 else piece == 2))
+            return (4 + piece, ROOT) if z else None
+        if y and (piece == 0 or not x):
+            up = y == 1 or (y == 2 and (x % 2 == 0 if piece == 0 else z == 0))
             return (2, (z, y - 1, x)) if up else (3, (z, (y + 1) % 4, x))
-        up = x == 1 or (x == 2 and (y % 2 == 0 if piece >= 2 else piece == 0))
+        up = x == 1 or (x == 2 and (y % 2 == 0 if piece == 1 else z == 0))
         return (0, (z, y, x - 1)) if up else (1, (z, y, (x + 1) % 4))
     for axis in ("zxy", "zyx", "xzy", "yzx")[piece]:
         if axis == "z" and z:
@@ -68,21 +68,21 @@
     steps += [("proj", (j,), (0 if j < 4 else 1,), 1.2, None) for j in range(8)]
     steps += [("ret", (t, h), (), 0.6, None) for t in range(LEN // BLOCK) for h in range(2)]
     for r in range(3):
-        steps += [("out", (1, r), (2,), 1.2, None), ("out", (0, r), (), 1.2, None), ("mid", (r,), (), 1.0, None)]
-    steps += [("pass", (i,), (), 0.1, (("mid", (i,)), 8.5 + 3.0 * i)) for i in range(3)]
-    steps += [("mlp", (2, i), (3,), 1.6, None) for i in range(2)]
-    steps += [("mlp", (3, i), (), 1.6, None) for i in range(2)]
-    tail = [("mlp", (0, i), (), 1.6, None) for i in range(2)] + [("mlp", (1, i), (), 1.6, None) for i in range(2)]
-    tail += [("own", (g,), (), 1.0, None) for g in range(8)]
-    for g in range(8):
-        steps += [("lent", (g,), (("g", g),), 1.2, None)] + (tail[g // 2 : g // 2 + 1] if g % 2 else [])
-    return steps + tail[4:]
+        steps += [("out", (1, r), (2,), 2.0, None), ("out", (0, r), (), 2.0, None), ("mid", (r,), (), 0.8, None)]
+    steps += [("first", (p, i), (3,), 0.9, None) for p in (0, 1) for i in range(2)]
+    steps += [("pass", (i,), (), 0.1, (("mid", (i,)), 7.0 + i)) for i in range(2)]
+    steps += [("first", (p, 0), (), 0.9, None) for p in (2, 3)]
+    steps += [("pass", (2,), (), 0.1, (("mid", (2,)), 9.0))]
+    steps += [("first", (p, 1), (), 0.9, None) for p in (2, 3)]
+    steps += [("rest", (p, i), (4,), 0.8, None) for p in (2, 3, 0, 1) for i in range(2)]
+    steps += [("lent", (g,), (("g", g),), 0.9, None) for g in range(8)]
+    return steps + [("own", (g,), (), 0.9, None) for g in range(8)]
 
 
 def program_order(steps, rate=47.0e3, latency=2.2, lead=LEAD):
     kids = {}
     for array in range(len(WIDTHS)):
-        for piece in range(PIECES):
+        for piece in range(PIECES[array]):
             for offset in OFFSETS[1:]:
                 d, above = parent(array, piece, offset)
                 kids.setdefault((array, piece, above), []).append((offset, d))
@@ -96,14 +96,14 @@
 
     def needs(dep):
         if isinstance(dep, tuple):
-            return [(LAST, p, o) for p in range(PIECES) for o in OFFSETS if o[:2] == GROUPS[dep[1]]]
-        return [(dep, p, o) for p in range(PIECES) for o in OFFSETS]
+            return [(LAST, p, o) for p in range(PIECES[LAST]) for o in OFFSETS if o[:2] == GROUPS[dep[1]]]
+        return [(dep, p, o) for p in range(PIECES[dep]) for o in OFFSETS]
 
     ready = [[] for _ in range(6)]
     free = [0.0] * 6
     coming, arrival = [], {}
     for array in range(len(WIDTHS)):
-        for piece in range(PIECES):
+        for piece in range(PIECES[array]):
             heapq.heappush(coming, (8.0 if array in SPLIT else 2.0, (array, piece, ROOT)))
     order, now, todo, done = [], 0.0, list(steps), {}
 
@@ -118,7 +118,7 @@
         for d in range(6):
             while ready[d] and free[d] - now < lead:
                 _, array, piece, child, offset = heapq.heappop(ready[d])
-                free[d] = max(free[d], now) + WIDTHS[array] * 2 * PIECE_ROWS / rate
+                free[d] = max(free[d], now) + WIDTHS[array] * 2 * ROWS / PIECES[array] / rate
                 heapq.heappush(coming, (free[d] + latency, (array, piece, child)))
                 order.append(("send", now, (d, array, piece, offset, child)))
                 now += 0.03
@@ -149,6 +149,25 @@
 ORDER, ARRIVAL, _, _ = program_order(STEPS)
 
 
+def semaphores():
+    slots, counts, onward = {}, {}, set()
+    for array in range(len(ARRAYS)):
+        for piece in range(PIECES[array]):
+            onward |= {(array, piece, parent(array, piece, offset)[1]) for offset in OFFSETS[1:]}
+    for array in range(len(ARRAYS)):
+        for piece in range(PIECES[array]):
+            for offset in OFFSETS[1:]:
+                key = (array, piece, offset)
+                if key not in onward:
+                    key = (array, offset[:2] if array == LAST else None)
+                counts[key] = counts.get(key, 0) + 1
+                slots.setdefault(key, len(slots))
+    return slots, counts
+
+
+SLOTS, COUNTS = semaphores()
+
+
 def tables():
     position = np.arange(LEN, dtype=np.float32)
     inverse = np.float32(1.0) / np.float32(rope_base) ** np.linspace(0.0, 1.0, DK // 2, dtype=np.float32)
@@ -203,29 +222,29 @@
     helper = {"rep": ze // 2, "fs_0": lax.rem(ze, 2)}
     helped = {"rep": zb // 2, "fs_0": lax.rem(zb, 2)}
 
-    here_m = pl.ds(pl.multiple_of(lo * (SIDE + TILE), TILE), SIDE)
-    here_d = pl.ds(pl.multiple_of((1 - lo) * (SIDE + TILE), TILE), SIDE)
-    tile = pl.ds(SIDE, TILE)
-    left, right = pl.ds(0, SIDE), pl.ds(SIDE + TILE, SIDE)
+    def columns_of(side, first, count):
+        return pl.ds(pl.multiple_of(side * (SIDE + TILE) + first, TILE), count)
+
+    tile, shared = pl.ds(SIDE, TILE), pl.ds(2 * SIDE - 256, TILE)
+    places = (((0, FIRST), 0, FIRST), ((FIRST, SIDE - FIRST), 2 * FIRST, 2 * FIRST + SIDE - FIRST + TILE))
     parts = {
         0: [(q_ref, wq.at[own, pl.ds(0, 512)]), (k_ref, wq.at[own, pl.ds(512, 512)])],
         1: [(v_ref, wq.at[own, pl.ds(1024, 1024)])],
         2: [(o_ref, wo.at[own, :])],
-        3: [
-            (g_ref.at[:, tile], mixed.at[0]),
-            (u_ref.at[:, tile], mixed.at[1]),
-            (g_ref.at[:, here_m], wm.at[own, left]),
-            (u_ref.at[:, here_m], wm.at[own, right]),
-            (g_ref.at[:, here_d], other_m.at[:, left]),
-            (u_ref.at[:, here_d], other_m.at[:, right]),
-        ],
-        4: [
-            (d_ref.at[:, here_m], wd.at[own, left]),
+        3: [],
+        4: [(g_ref.at[:, tile], mixed.at[0]), (u_ref.at[:, tile], mixed.at[1])],
+        5: [
+            (d_ref.at[:, columns_of(lo, 0, SIDE)], wd.at[own, pl.ds(0, SIDE)]),
             (d_ref.at[:, tile], wd.at[own, tile]),
-            (d_ref.at[:, here_d], other_d.at[:, left]),
+            (d_ref.at[:, columns_of(1 - lo, 0, SIDE)], other_d.at[:, pl.ds(0, SIDE)]),
             (d_ref.at[:, tile], other_d.at[:, tile]),
         ],
     }
+    for array, (span, gate_at, up_at) in zip((3, 4), places):
+        for ref, at in ((g_ref, gate_at), (u_ref, up_at)):
+            there = pl.ds(at, span[1])
+            parts[array].append((ref.at[:, columns_of(lo, *span)], wm.at[own, there]))
+            parts[array].append((ref.at[:, columns_of(1 - lo, *span)], other_m.at[:, there]))
     fills = {}
     for array, pairs in parts.items():
         fills[array] = []
@@ -233,7 +252,7 @@
             at = sum(len(f) for f in fills.values())
             fills[array].append(pltpu.make_async_copy(source, there, local.at[at]))
             fills[array][-1].start()
-    fill = pltpu.make_async_copy(resid, rows_in.at[pl.ds(mine, HALF), :], local.at[15])
+    fill = pltpu.make_async_copy(resid, rows_in.at[pl.ds(mine, HALF), :], local.at[18])
     fill.start()
     pl.semaphore_wait(barrier, 7)
 
@@ -252,16 +271,18 @@
 
     def chunk(array, piece, offset):
         buffer, first, width = ARRAYS[array]
-        start = pl.multiple_of(base(offset) + piece * PIECE_ROWS, PIECE_ROWS)
-        return buffers[buffer].at[pl.ds(start, PIECE_ROWS), pl.ds(first, width)]
-
-    def slot_of(array, piece, offset):
-        return (array * PIECES + piece) * len(OFFSETS) + OFFSETS.index(offset)
+        count = ROWS // PIECES[array]
+        start = pl.multiple_of(base(offset) + piece * count, count)
+        return buffers[buffer].at[pl.ds(start, count), pl.ds(first, width)]
+
+    def key_of(array, piece, offset):
+        whole = (array, piece, offset)
+        return whole if whole in SLOTS else (array, offset[:2] if array == LAST else None)
 
     waited = set()
 
     def arrive(array, piece, offset):
-        key = (array,) if offset == ROOT else (array, piece, offset)
+        key = (array,) if offset == ROOT else key_of(array, piece, offset)
         if key in waited:
             return
         waited.add(key)
@@ -269,16 +290,18 @@
             for item in fills[array]:
                 item.wait()
         else:
-            here = chunk(array, piece, offset)
-            pltpu.make_async_copy(here, here, recv.at[slot_of(array, piece, offset)]).wait()
+            buffer, first, width = ARRAYS[array]
+            all_rows = COUNTS[key] * ROWS // PIECES[array]
+            here = buffers[buffer].at[pl.ds(0, all_rows), pl.ds(first, width)]
+            pltpu.make_async_copy(here, here, recv.at[SLOTS[key]]).wait()
 
     def prepare():
-        arrive(3, 0, ROOT)
+        arrive(4, 0, ROOT)
         lane = lax.broadcasted_iota(jnp.int32, (ROWS, TILE), 1) // (TILE // 2)
         gate = mixed[0].astype(F32)
         up = pltpu.roll(mixed[1].astype(F32), TILE // 2, 1)
-        wm[own, tile] = jnp.where(lane == lo, gate, up).astype(BF16)
-        other_m[:, tile] = jnp.where(lane == 1 - lo, gate, up).astype(BF16)
+        wm[own, shared] = jnp.where(lane == lo, gate, up).astype(BF16)
+        other_m[:, shared] = jnp.where(lane == 1 - lo, gate, up).astype(BF16)
 
     def norm_rows(source, gain, start, count):
         def some(i, _):
@@ -387,30 +410,32 @@
 
     quarter = HALF // 2
 
-    def expand(part, i):
-        if (part, i) == (1, 0):
-            for r in range(3):
-                swaps[5 + r].wait()
-        if (part, i) == (3, 0):
-            for r in range(3):
-                swaps[8 + r].wait()
+    def rows_of(part, i):
         side = core if part % 2 == 0 else 1 - core
         if part < 2:
             source = normed[pl.ds(pl.multiple_of(side * HALF + i * quarter, quarter), quarter), :]
         else:
             source = foreign[side, pl.ds(i * quarter, quarter), :]
-        both = jnp.dot(source, wm[...], preferred_element_type=F32)
-        place = 2 * (part // 2) + side
-        rows = pl.ds(i * quarter, quarter)
-        hidden[place, rows, pl.ds(0, SIDE)] = (
-            jax.nn.silu(both[:, :SIDE]) * both[:, SIDE + TILE :]
+        return source, 2 * (part // 2) + side, pl.ds(i * quarter, quarter)
+
+    def expand_first(part, i):
+        for r in {(1, 0): (5, 6, 7), (3, 0): (8, 9), (3, 1): (10,)}.get((part, i), ()):
+            swaps[r].wait()
+        source, place, rows = rows_of(part, i)
+        both = jnp.dot(source, wm[:, pl.ds(0, 2 * FIRST)], preferred_element_type=F32)
+        hidden[place, rows, pl.ds(0, FIRST)] = (jax.nn.silu(both[:, :FIRST]) * both[:, FIRST:]).astype(BF16)
+
+    def expand_rest(part, i):
+        source, place, rows = rows_of(part, i)
+        count = SIDE - FIRST
+        both = jnp.dot(source, wm[:, pl.ds(2 * FIRST, 2 * count + TILE)], preferred_element_type=F32)
+        hidden[place, rows, pl.ds(FIRST, count)] = (
+            jax.nn.silu(both[:, :count]) * both[:, count + TILE :]
         ).astype(BF16)
-        shared = both[:, SIDE : SIDE + TILE]
-        found = jax.nn.silu(shared) * pltpu.roll(shared, TILE // 2, 1)
+        pair = both[:, count : count + TILE]
+        found = jax.nn.silu(pair) * pltpu.roll(pair, TILE // 2, 1)
         lane = lax.broadcasted_iota(jnp.int32, (quarter, TILE), 1) // (TILE // 2)
         hidden[place, rows, tile] = jnp.where(lane == lo, found, 0.0).astype(BF16)
-        if part < 2:
-            send_back()
 
     blocks = {}
 
@@ -481,7 +506,7 @@
 
     run = {
         "prep": prepare, "norm": norm, "proj": project, "ret": retain, "out": give_heads,
-        "mid": middle, "pass": forward, "mlp": expand, "lent": lent, "own": own_rows,
+        "mid": middle, "pass": forward, "first": expand_first, "rest": expand_rest, "lent": lent, "own": own_rows,
     }
     for name, _, what in ORDER:
         if name == "send":
@@ -489,18 +514,20 @@
             arrive(array, piece, offset)
             source = here = chunk(array, piece, offset)
             if array in SPLIT and child == (1, 0, 0):
-                source = (other_m, other_d)[array - 3].at[pl.ds(piece * PIECE_ROWS, PIECE_ROWS), :]
+                buffer, first, width = ARRAYS[array]
+                count = ROWS // PIECES[array]
+                source = (other_m, other_d)[buffer - 2].at[pl.ds(piece * count, count), pl.ds(first, width)]
             pltpu.make_async_remote_copy(
                 src_ref=source,
                 dst_ref=here,
                 send_sem=send.at[array],
-                recv_sem=recv.at[slot_of(array, piece, child)],
+                recv_sem=recv.at[SLOTS[key_of(array, piece, child)]],
                 device_id=peers[d],
                 device_id_type=MESH_ID,
             ).start()
         else:
             args, wanted = what
-            for item in wanted:
+            for item in sorted(wanted, key=lambda c: key_of(*c) in COUNTS and COUNTS[key_of(*c)] > 1):
                 arrive(*item)
             run[name](*args)
     send_back()
@@ -528,10 +555,10 @@
         scratch_shapes=[
             pltpu.VMEM((D, 2048), BF16),
             pltpu.VMEM((D, 1024), BF16),
-            pltpu.VMEM((D, ARRAYS[3][2]), BF16),
-            pltpu.VMEM((D, ARRAYS[4][2]), BF16),
-            pltpu.VMEM((ROWS, ARRAYS[3][2]), BF16),
-            pltpu.VMEM((ROWS, ARRAYS[4][2]), BF16),
+            pltpu.VMEM((D, 2 * SIDE + TILE), BF16),
+            pltpu.VMEM((D, SIDE + TILE), BF16),
+            pltpu.VMEM((ROWS, 2 * SIDE + TILE), BF16),
+            pltpu.VMEM((ROWS, SIDE + TILE), BF16),
             pltpu.VMEM((2, ROWS, TILE), BF16),
             pltpu.VMEM((LEN, D), BF16),
             pltpu.VMEM((LEN, D), BF16),
@@ -545,9 +572,9 @@
         + [pltpu.VMEM((8, 2, 2, HALF, 256), BF16), pltpu.VMEM((8, 2, HALF, 256), BF16)]
         + [pltpu.VMEM((8, HALF, 256), BF16)] * 2
         + [
-            pltpu.SemaphoreType.DMA((len(ARRAYS) * PIECES * len(OFFSETS),)),
+            pltpu.SemaphoreType.DMA((len(SLOTS),)),
             pltpu.SemaphoreType.DMA((len(ARRAYS),)),
-            pltpu.SemaphoreType.DMA((16,)),
+            pltpu.SemaphoreType.DMA((19,)),
             pltpu.SemaphoreType.DMA((38,)),
             pltpu.SemaphoreType.DMA((38,)),
             pltpu.SemaphoreType.DMA((8,)),

time: 129 us -> 127 us (0.984)
  Pallas kernels: 126 us -> 124 us
    pallas_call x1, Pallas kernels: 126 us -> 124 us  [shards(): pl.pallas_call(layer_kernel, out_shape=jax.ShapeDtypeStruct((HALF, D), BF...]
where the time goes in v5:
time: 127 us
  Pallas kernels  124 us (98%)
  local copies, waits for them, and re-layouts  2.73 us (2%)
    pallas_call x1, Pallas kernels, shards(): pl.pallas_call(layer_kernel, out_shape=jax.ShapeDtypeStruct((HALF, D), BF...  124 us
    unnamed x1, local copies, waits for them, and re-layouts  2.73 us

profile of v5, /device:TPU:1, one launch (start us, length us, event | category | flops | bytes accessed | tf_op | source)
XLA Modules:
  0.0 127.0 jit_solution(15778914147964630873)
XLA Ops:
  0.0 124.3 %shard_map.154 = bf16[384,2048]{1,0:T(8,128)(2,1)} custom-call(bf16[384,2048]{1,0:T(8,128)(2,1)} %resid.1, f32[1,2048]{1,0:T(1,128)} %bitcast.7, bf16[64,512]{1,0:T(8,128)(2,1)} %q_ref.1, bf16[64,512]{1,0:T(8,128)(2,1)} %k_ref.1, bf16[64,1024]{1,0:T(8,128)(2,1)} %v_ref.1, f32[1,1024]{1,0:T(1,128)} %bitcast.9, bf16[64,1024]{1,0:T(8,128)(2,1)} %bitcast.6, ...), custom_call_target="tpu_custom_call" | custom-call | tf_op jit(solution)/shard_map/pallas_call | solution.py:549
  124.3 2.7 %copy.18 = bf16[384,2048]{1,0:T(8,128)(2,1)} copy(bf16[384,2048]{1,0:T(8,128)(2,1)} %shard_map.154) | data formatting | bytes 3145728

commit v6 on v5

--- a/solution.py
+++ b/solution.py
@@ -28,8 +28,11 @@
 WIDTHS = tuple(width for _, _, width in ARRAYS)
 LAST = len(ARRAYS) - 1
 SPLIT = (3, 4, 5)
-DUE = (20, 25, 30, 66, 78, 86)
+EVEN = ("zxy", "zyx", "xzy", "yzx")
+TREES = (EVEN, EVEN, EVEN)
+DUE = (20, 25, 30, 70, 72, 110)
 HOP = 4.0
+CROSS = 30.0
 LEAD = 4.0
 OFFSETS = [(z, y, x) for z in range(2) for y in range(4) for x in range(4)]
 GROUPS = [(z, y) for y in (0, 1, 3, 2) for z in range(2)]
@@ -51,7 +54,7 @@
             return (2, (z, y - 1, x)) if up else (3, (z, (y + 1) % 4, x))
         up = x == 1 or (x == 2 and (y % 2 == 0 if piece == 1 else z == 0))
         return (0, (z, y, x - 1)) if up else (1, (z, y, (x + 1) % 4))
-    for axis in ("zxy", "zyx", "xzy", "yzx")[piece]:
+    for axis in TREES[array][piece]:
         if axis == "z" and z:
             return 4 + (x + y + piece) % 2, (0, y, x)
         if axis == "x" and x:
@@ -69,13 +72,14 @@
     steps += [("ret", (t, h), (), 0.6, None) for t in range(LEN // BLOCK) for h in range(2)]
     for r in range(3):
         steps += [("out", (1, r), (2,), 2.0, None), ("out", (0, r), (), 2.0, None), ("mid", (r,), (), 0.8, None)]
-    steps += [("first", (p, i), (3,), 0.9, None) for p in (0, 1) for i in range(2)]
-    steps += [("pass", (i,), (), 0.1, (("mid", (i,)), 7.0 + i)) for i in range(2)]
-    steps += [("first", (p, 0), (), 0.9, None) for p in (2, 3)]
-    steps += [("pass", (2,), (), 0.1, (("mid", (2,)), 9.0))]
-    steps += [("first", (p, 1), (), 0.9, None) for p in (2, 3)]
-    steps += [("rest", (p, i), (4,), 0.8, None) for p in (2, 3, 0, 1) for i in range(2)]
-    steps += [("lent", (g,), (("g", g),), 0.9, None) for g in range(8)]
+    own = [("first", (p, i), (3,), 1.0, None) for p in (0, 1) for i in range(2)]
+    passes = [("pass", (i,), (), 0.1, (("mid", (i,)), 7.0 + i)) for i in range(3)]
+    steps += passes[:2] + [("first", (p, 0), (3,), 1.0, None) for p in (2, 3)] + own + passes[2:]
+    steps += [("first", (p, 1), (), 1.0, None) for p in (2, 3)]
+    steps += [("rest", (p, i), (4,), 0.9, None) for p in (2, 3) for i in range(2)]
+    own = [("rest", (p, i), (), 0.9, None) for p in (0, 1) for i in range(2)]
+    for g in range(8):
+        steps += [("lent", (g,), (("g", g),), 1.1, None)] + own[g : g + 1]
     return steps + [("own", (g,), (), 0.9, None) for g in range(8)]
 
 
@@ -91,6 +95,8 @@
         return max([0] + [1 + depth(*at[:2], c) for c, _ in kids.get(at, [])])
 
     def due(array, piece, child):
+        if array in SPLIT and child == (1, 0, 0):
+            return CROSS
         late = GROUPS.index(child[:2]) if array == LAST else 0
         return DUE[array] + late - HOP * depth(array, piece, child)
 
@@ -260,7 +266,7 @@
         return pltpu.make_async_remote_copy(
             src_ref=source,
             dst_ref=there,
-            send_sem=swap_send.at[slot],
+            send_sem=swap_send.at[0 if slot < 11 else 1],
             recv_sem=swap_recv.at[slot],
             device_id=device,
             device_id_type=MESH_ID,
@@ -316,7 +322,7 @@
         if which == 0:
             fill.wait()
         else:
-            swaps[0].wait()
+            swaps[0].wait_recv()
         norm_rows(rows_in, mix_gain, half[which], HALF)
 
     def project(j):
@@ -387,7 +393,7 @@
         swaps[5 + r].start()
 
     def middle(r):
-        swaps[35 + r].wait()
+        swaps[35 + r].wait_recv()
 
         def some(i, _):
             here = pl.ds(pl.multiple_of(r * third + i * 32, 32), 32)
@@ -403,7 +409,7 @@
         lend(r)
 
     def forward(i):
-        swaps[2 + i].wait()
+        swaps[2 + i].wait_recv()
         here = foreign.at[core, pl.ds(i * third, third), :]
         swaps[8 + i] = swap(here, here, 8 + i)
         swaps[8 + i].start()
@@ -420,7 +426,7 @@
 
     def expand_first(part, i):
         for r in {(1, 0): (5, 6, 7), (3, 0): (8, 9), (3, 1): (10,)}.get((part, i), ()):
-            swaps[r].wait()
+            swaps[r].wait_recv()
         source, place, rows = rows_of(part, i)
         both = jnp.dot(source, wm[:, pl.ds(0, 2 * FIRST)], preferred_element_type=F32)
         hidden[place, rows, pl.ds(0, FIRST)] = (jax.nn.silu(both[:, :FIRST]) * both[:, FIRST:]).astype(BF16)
@@ -436,6 +442,7 @@
         found = jax.nn.silu(pair) * pltpu.roll(pair, TILE // 2, 1)
         lane = lax.broadcasted_iota(jnp.int32, (quarter, TILE), 1) // (TILE // 2)
         hidden[place, rows, tile] = jnp.where(lane == lo, found, 0.0).astype(BF16)
+        send_back()
 
     blocks = {}
 
@@ -457,7 +464,7 @@
 
     def send_back():
         for g in pending:
-            swaps[11 + g].wait()
+            swaps[11 + g].wait_recv()
             block = blocks[g]
 
             def some(i, _, block=block):
@@ -485,12 +492,11 @@
 
     def writing(g):
         place = result.at[:, pl.ds(pl.multiple_of(blocks[g] * 256, 256), 256)]
-        return pltpu.make_async_copy(both2.at[blocks[g], 0, 1], place, put.at[g])
+        return pltpu.make_async_copy(both2.at[blocks[g], 0, 1], place, put.at[0])
 
     def finish(g):
         block = blocks[g]
-        swaps[27 + g].wait()
-        swaps[19 + g].wait_send()
+        swaps[27 + g].wait_recv()
         swap(sums.at[block], back.at[block], 19 + (g ^ 1), helped).wait_recv()
 
         def some(i, _):
@@ -536,8 +542,9 @@
     for array, (buffer, first, width) in enumerate(ARRAYS):
         sent = buffers[buffer].at[pl.ds(0, 31 * ROWS), pl.ds(first, width)]
         pltpu.make_async_copy(sent, sent, send.at[array]).wait()
-    for g in range(len(GROUPS)):
-        writing(g).wait()
+    for slot in range(2):
+        pltpu.make_async_copy(both2, both2, swap_send.at[slot]).wait()
+    pltpu.make_async_copy(result, result, put.at[0]).wait()
 
 
 def shards(
@@ -575,9 +582,9 @@
             pltpu.SemaphoreType.DMA((len(SLOTS),)),
             pltpu.SemaphoreType.DMA((len(ARRAYS),)),
             pltpu.SemaphoreType.DMA((19,)),
+            pltpu.SemaphoreType.DMA((2,)),
             pltpu.SemaphoreType.DMA((38,)),
-            pltpu.SemaphoreType.DMA((38,)),
-            pltpu.SemaphoreType.DMA((8,)),
+            pltpu.SemaphoreType.DMA((1,)),
         ],
         compiler_params=pltpu.CompilerParams(
             collective_id=0, has_side_effects=True, vmem_limit_bytes=67043328

time: 127 us -> 123 us (0.969)
  Pallas kernels: 124 us -> 120 us
    pallas_call x1, Pallas kernels: 124 us -> 120 us  [shards(): pl.pallas_call(layer_kernel, out_shape=jax.ShapeDtypeStruct((HALF, D), BF...]
where the time goes in v6:
time: 123 us
  Pallas kernels  120 us (98%)
  local copies, waits for them, and re-layouts  2.73 us (2%)
    pallas_call x1, Pallas kernels, shards(): pl.pallas_call(layer_kernel, out_shape=jax.ShapeDtypeStruct((HALF, D), BF...  120 us
    unnamed x1, local copies, waits for them, and re-layouts  2.73 us

profile of v6, /device:TPU:1, one launch (start us, length us, event | category | flops | bytes accessed | tf_op | source)
XLA Modules:
  0.0 123.0 jit_solution(14718977948590895188)
XLA Ops:
  0.0 120.3 %shard_map.154 = bf16[384,2048]{1,0:T(8,128)(2,1)} custom-call(bf16[384,2048]{1,0:T(8,128)(2,1)} %resid.1, f32[1,2048]{1,0:T(1,128)} %bitcast.7, bf16[64,512]{1,0:T(8,128)(2,1)} %q_ref.1, bf16[64,512]{1,0:T(8,128)(2,1)} %k_ref.1, bf16[64,1024]{1,0:T(8,128)(2,1)} %v_ref.1, f32[1,1024]{1,0:T(1,128)} %bitcast.9, bf16[64,1024]{1,0:T(8,128)(2,1)} %bitcast.6, ...), custom_call_target="tpu_custom_call" | custom-call | tf_op jit(solution)/shard_map/pallas_call | solution.py:556
  120.3 2.7 %copy.18 = bf16[384,2048]{1,0:T(8,128)(2,1)} copy(bf16[384,2048]{1,0:T(8,128)(2,1)} %shard_map.154) | data formatting | bytes 3145728

commit v7 on v6

--- a/solution.py
+++ b/solution.py
@@ -22,18 +22,18 @@
 ROWS = 64
 SIDE = 640
 TILE = 128
-FIRST = 384
-ARRAYS = ((0, 0, 1024), (0, 1024, 1024), (1, 0, 1024), (2, 0, 2 * FIRST), (2, 2 * FIRST, 640), (3, 0, SIDE + TILE))
+FIRST = 256
+ARRAYS = ((0, 0, 1024), (0, 1024, 1024), (1, 0, 1024), (2, 0, 2 * FIRST), (2, 2 * FIRST, 2 * (SIDE - FIRST) + TILE), (3, 0, SIDE + TILE))
 PIECES = (4, 4, 4, 2, 2, 2)
 WIDTHS = tuple(width for _, _, width in ARRAYS)
 LAST = len(ARRAYS) - 1
 SPLIT = (3, 4, 5)
 EVEN = ("zxy", "zyx", "xzy", "yzx")
 TREES = (EVEN, EVEN, EVEN)
-DUE = (20, 25, 30, 70, 72, 110)
+DUE = (20, 25, 30, 60, 60, 85)
 HOP = 4.0
 CROSS = 30.0
-LEAD = 4.0
+LEAD = 3.0
 OFFSETS = [(z, y, x) for z in range(2) for y in range(4) for x in range(4)]
 GROUPS = [(z, y) for y in (0, 1, 3, 2) for z in range(2)]
 ROOT = (0, 0, 0)
@@ -72,18 +72,20 @@
     steps += [("ret", (t, h), (), 0.6, None) for t in range(LEN // BLOCK) for h in range(2)]
     for r in range(3):
         steps += [("out", (1, r), (2,), 2.0, None), ("out", (0, r), (), 2.0, None), ("mid", (r,), (), 0.8, None)]
-    own = [("first", (p, i), (3,), 1.0, None) for p in (0, 1) for i in range(2)]
-    passes = [("pass", (i,), (), 0.1, (("mid", (i,)), 7.0 + i)) for i in range(3)]
-    steps += passes[:2] + [("first", (p, 0), (3,), 1.0, None) for p in (2, 3)] + own + passes[2:]
-    steps += [("first", (p, 1), (), 1.0, None) for p in (2, 3)]
-    steps += [("rest", (p, i), (4,), 0.9, None) for p in (2, 3) for i in range(2)]
-    own = [("rest", (p, i), (), 0.9, None) for p in (0, 1) for i in range(2)]
+    def part(name, parts, half, us, deps=()):
+        return [(name, (p, i), deps, us, None) for p in parts for i in half]
+
+    passes = [("pass", (i,), (), 0.1, (("mid", (i,)), (7.0, 8.3, 8.5)[i])) for i in range(3)]
+    steps += passes[:1] + part("first", (0, 1), (0, 1), 0.8, (3,)) + passes[1:2]
+    steps += part("first", (2, 3), (0,), 0.8) + passes[2:] + part("first", (2, 3), (1,), 0.9)
+    steps += part("rest", (2, 3), (0, 1), 1.05, (4,))
+    own = part("rest", (0, 1), (0, 1), 1.05)
     for g in range(8):
         steps += [("lent", (g,), (("g", g),), 1.1, None)] + own[g : g + 1]
     return steps + [("own", (g,), (), 0.9, None) for g in range(8)]
 
 
-def program_order(steps, rate=47.0e3, latency=2.2, lead=LEAD):
+def program_order(steps, rate=46.0e3, latency=2.2, lead=LEAD):
     kids = {}
     for array in range(len(WIDTHS)):
         for piece in range(PIECES[array]):
@@ -231,7 +233,7 @@
     def columns_of(side, first, count):
         return pl.ds(pl.multiple_of(side * (SIDE + TILE) + first, TILE), count)
 
-    tile, shared = pl.ds(SIDE, TILE), pl.ds(2 * SIDE - 256, TILE)
+    tile, shared = pl.ds(SIDE, TILE), pl.ds(SIDE + FIRST, TILE)
     places = (((0, FIRST), 0, FIRST), ((FIRST, SIDE - FIRST), 2 * FIRST, 2 * FIRST + SIDE - FIRST + TILE))
     parts = {
         0: [(q_ref, wq.at[own, pl.ds(0, 512)]), (k_ref, wq.at[own, pl.ds(512, 512)])],

time: 123 us -> 121 us (0.984)
    pallas_call x1, Pallas kernels: 120 us -> 119 us  [shards(): pl.pallas_call(layer_kernel, out_shape=jax.ShapeDtypeStruct((HALF, D), BF...]
where the time goes in v7:
time: 121 us
  Pallas kernels  119 us (98%)
  local copies, waits for them, and re-layouts  2.73 us (2%)
    pallas_call x1, Pallas kernels, shards(): pl.pallas_call(layer_kernel, out_shape=jax.ShapeDtypeStruct((HALF, D), BF...  119 us
    unnamed x1, local copies, waits for them, and re-layouts  2.73 us

profile of v7, /device:TPU:1, one launch (start us, length us, event | category | flops | bytes accessed | tf_op | source)
XLA Modules:
  0.0 121.3 jit_solution(11008635088923211137)
XLA Ops:
  0.0 118.6 %shard_map.154 = bf16[384,2048]{1,0:T(8,128)(2,1)} custom-call(bf16[384,2048]{1,0:T(8,128)(2,1)} %resid.1, f32[1,2048]{1,0:T(1,128)} %bitcast.7, bf16[64,512]{1,0:T(8,128)(2,1)} %q_ref.1, bf16[64,512]{1,0:T(8,128)(2,1)} %k_ref.1, bf16[64,1024]{1,0:T(8,128)(2,1)} %v_ref.1, f32[1,1024]{1,0:T(1,128)} %bitcast.9, bf16[64,1024]{1,0:T(8,128)(2,1)} %bitcast.6, ...), custom_call_target="tpu_custom_call" | custom-call | tf_op jit(solution)/shard_map/pallas_call | solution.py:558
  118.6 2.7 %copy.18 = bf16[384,2048]{1,0:T(8,128)(2,1)} copy(bf16[384,2048]{1,0:T(8,128)(2,1)} %shard_map.154) | data formatting | bytes 3145728
